TPU v7x, 128 devices: a whole 4x4x4 slice. The times are simulated.
128 devices in a mesh: sp: 16 (over z, y), tp: 8 (over x, core).
Axes of the slice: x: 4, y: 4, z: 4, core: 2. Of those that a mesh axis runs over, the one named last changes fastest.
Arguments:
- latents: bfloat16 [4096, 4096], P('sp'), may hold values from -0.4375 to 0.4375
- query_heads: bfloat16 [4096, 16, 128], P('sp', 'tp'), may hold values from -8 to 8
- key_heads: bfloat16 [4096, 16, 128], P('sp', 'tp'), may hold values from -8 to 8
- value_heads: bfloat16 [4096, 16, 128], P('sp', 'tp'), may hold values from -6 to 6
- map_outputs: bfloat16 [4096, 2, 16, 128], P('sp', None, 'tp'), may hold values from -6 to 6
- log_sums: float32 [4096, 16, 2], P('sp', 'tp'), may hold values from -600 to 600, as said below
- out_grad: bfloat16 [4096, 16, 128], P('sp', 'tp'), may hold values from -6 to 6
- mix_lambda: float32 [16], P('tp'), may hold values from 0.3 to 0.8
- norm_gain: float32 [128], replicated, may hold values from 0.1 to 1.9
Outputs:
- query_grad: bfloat16 [4096, 16, 128], P('sp', 'tp')
- key_grad: bfloat16 [4096, 16, 128], P('sp', 'tp')
- value_grad: bfloat16 [4096, 16, 128], P('sp', 'tp')
- weight_grad: float32 [4096, 2048], P('sp', 'tp')
Inputs may be any that keep to these rules, and one draw needn't show every extreme that they name: query_heads, key_heads and value_heads together with map_outputs and log_sums are one consistent causal forward pass: log_sums is the row's log-sum of exp(score_m) over keys at or before the row, and map_outputs[:, m] is prob_m times value_heads rounded to bfloat16.
All inputs are finite; a program needn't handle non-finite values.
Results may differ from a plain program's by a relative error of at most 0.019.
Values may be sent and summed in bfloat16 or wider, within the bound.
A program may use at most 64 MiB of HBM per device.

v0:
```python
import jax
import jax.numpy as jnp
from jax import lax
from jax.sharding import PartitionSpec as P

DH = 64


EPSILON = 1e-05


def joined_along(blocks, dim):
    blocks = jnp.moveaxis(blocks, 0, dim)
    lengths = blocks.shape
    return blocks.reshape(*lengths[:dim], lengths[dim] * lengths[dim + 1], *lengths[dim + 2 :])


def from_everyone(shard, axis):
    devices = lax.axis_size(axis)
    return lax.all_to_all(
        jnp.broadcast_to(shard[None], (devices, *shard.shape)), axis, 0, 0, tiled=True
    )


def collect(shard, axis, dim):
    return joined_along(from_everyone(shard, axis), dim)


def side_by_side(arrays, axis, dim, along):
    widths = [a.shape[along] for a in arrays]
    both = jnp.concatenate(arrays, axis=along)
    result = lax.all_gather(both, axis, axis=dim, tiled=True)
    return tuple(jnp.split(result, [sum(widths[:k]) for k in range(1, len(widths))], axis=along))


def split_up(shard, dim, devices):
    lengths = shard.shape
    blocks = shard.reshape(*lengths[:dim], devices, lengths[dim] // devices, *lengths[dim + 1 :])
    return jnp.moveaxis(blocks, dim, 0)


def sent_and_summed(shard, axis, dim):
    blocks = split_up(shard, dim, lax.axis_size(axis))
    arrived = lax.all_to_all(blocks, axis, split_axis=0, concat_axis=0, tiled=True)
    return arrived.astype(jnp.float32).sum(axis=0)


def norm_backward(map_outputs, out_grad, mix_lambda, norm_gain):
    first_map = map_outputs[:, 0].astype(jnp.float32)
    second_map = map_outputs[:, 1].astype(jnp.float32)
    lambda_col = mix_lambda[None, :, None]
    combined = first_map - lambda_col * second_map
    inverse = lax.rsqrt(jnp.mean(combined * combined, axis=-1, keepdims=True) + EPSILON)
    weighted = norm_gain[None, None, :] * out_grad.astype(jnp.float32)
    grad_out = (
        inverse * weighted
        - inverse**3 * combined * jnp.mean(combined * weighted, axis=-1, keepdims=True)
    ).astype(jnp.bfloat16)
    grad_wide = grad_out.astype(jnp.float32)
    row_terms = jnp.stack(
        [jnp.sum(grad_wide * first_map, axis=-1), jnp.sum(grad_wide * second_map, axis=-1)], axis=-1
    )
    return (grad_out, row_terms)


def block_grads(
    query_blk, grad_blk, lse_blk, term_blk, key_blk, value_blk, query_pos, key_pos, mix_lambda
):
    row_count = query_blk.shape[0]
    col_count = key_blk.shape[0]
    head_count = query_blk.shape[1]
    score_scale = DH ** (-0.5)
    query_split = query_blk.reshape(row_count, head_count, 2, DH)
    key_split = key_blk.reshape(col_count, head_count, 2, DH)
    scores = (
        jnp.einsum("qhmd,khmd->hmqk", query_split, key_split, preferred_element_type=jnp.float32)
        * score_scale
    )
    causal = key_pos[None, :] <= query_pos[:, None]
    softmax_maps = jnp.exp(
        jnp.where(causal, scores - jnp.transpose(lse_blk, (1, 2, 0))[..., None], -jnp.inf)
    )
    mixed_grad = jnp.einsum("qhe,khe->hqk", grad_blk, value_blk, preferred_element_type=jnp.float32)
    map_signs = jnp.stack([jnp.ones_like(mix_lambda), -mix_lambda], axis=1)[:, :, None, None]
    score_grad = (
        map_signs
        * softmax_maps
        * (mixed_grad[:, None] - jnp.transpose(term_blk, (1, 2, 0))[..., None])
    ).astype(jnp.bfloat16)
    diff_weights = (softmax_maps[:, 0] - mix_lambda[:, None, None] * softmax_maps[:, 1]).astype(
        jnp.bfloat16
    )
    value_part = jnp.einsum(
        "hqk,qhe->khe", diff_weights, grad_blk, preferred_element_type=jnp.float32
    )
    query_part = score_scale * jnp.einsum(
        "hmqk,khmd->qhmd", score_grad, key_split, preferred_element_type=jnp.float32
    )
    key_part = score_scale * jnp.einsum(
        "hmqk,qhmd->khmd", score_grad, query_split, preferred_element_type=jnp.float32
    )
    return (
        query_part.reshape(row_count, head_count, 2 * DH),
        key_part.reshape(col_count, head_count, 2 * DH),
        value_part,
    )


def add_rows(buffer, anchor, addition):
    length = addition.shape[0]
    current = lax.dynamic_slice_in_dim(buffer, anchor, length, 0)
    return lax.dynamic_update_slice_in_dim(buffer, current + addition, anchor, 0)


def unchanged(running):
    return running


def body(
    latents,
    query_heads,
    key_heads,
    value_heads,
    map_outputs,
    log_sums,
    out_grad,
    mix_lambda,
    norm_gain,
):
    rows_dev = query_heads.shape[0]
    head_count = query_heads.shape[1]
    width = query_heads.shape[2]
    seq_total = rows_dev * lax.axis_size("sp")
    offset = lax.axis_index("sp") * rows_dev
    own_pos = offset + jnp.arange(rows_dev, dtype=jnp.int32)
    grad_out, row_terms = norm_backward(map_outputs, out_grad, mix_lambda, norm_gain)
    local_zero = jnp.zeros((rows_dev, head_count, width), jnp.float32)
    global_zero = jnp.zeros((seq_total, head_count, width), jnp.float32)
    row_stats = jnp.concatenate([log_sums, row_terms], axis=-1)
    all_stats = collect(row_stats, "sp", 0)
    query_piece, grad_piece = side_by_side((query_heads, grad_out), "sp", 0, 1)
    pieces = query_piece.shape[0] // rows_dev
    blocks = (
        query_piece.reshape(pieces, rows_dev, head_count, width),
        grad_piece.reshape(pieces, rows_dev, head_count, width),
        jnp.arange(pieces, dtype=jnp.int32),
    )

    def visit(state, element):
        query_blk, grad_blk, block_index = element
        first_query = block_index * rows_dev

        def accumulate(inner):
            query_term, key_acc, value_acc = inner
            query_pos = first_query + jnp.arange(rows_dev, dtype=jnp.int32)
            stats_blk = lax.dynamic_slice_in_dim(all_stats, first_query, rows_dev, 0)
            query_part, key_part, value_part = block_grads(
                query_blk,
                grad_blk,
                stats_blk[..., :2],
                stats_blk[..., 2:],
                key_heads,
                value_heads,
                query_pos,
                own_pos,
                mix_lambda,
            )
            return (
                add_rows(query_term, first_query, query_part),
                key_acc + key_part,
                value_acc + value_part,
            )

        return (lax.cond(first_query + rows_dev > offset, accumulate, unchanged, state), None)

    result, _ = lax.scan(visit, (global_zero, local_zero, local_zero), blocks)
    query_term, key_acc, value_acc = result
    query_acc = sent_and_summed(query_term.astype(jnp.bfloat16), "sp", 0)
    query_grad = query_acc.astype(jnp.bfloat16)
    flat_grad = query_grad.reshape(rows_dev, head_count * width)
    weight_grad = sent_and_summed(
        lax.dot_general(
            latents, flat_grad, (((0,), (0,)), ((), ())), preferred_element_type=jnp.float32
        ).astype(jnp.bfloat16),
        "sp",
        0,
    )
    return (query_grad, key_acc.astype(jnp.bfloat16), value_acc.astype(jnp.bfloat16), weight_grad)


def solution(mesh):
    placed = (
        P("sp", None),
        P("sp", "tp", None),
        P("sp", "tp", None),
        P("sp", "tp", None),
        P("sp", None, "tp", None),
        P("sp", "tp", None),
        P("sp", "tp", None),
        P("tp"),
        P(),
    )
    return jax.shard_map(
        body,
        mesh=mesh,
        in_specs=placed,
        out_specs=(P("sp", "tp", None), P("sp", "tp", None), P("sp", "tp", None), P("sp", "tp")),
        check_vma=False,
    )
```

profile of v0, /device:TPU:0, one launch (start us, length us, event | category | flops | bytes accessed | tf_op | source)
XLA Modules:
  0.0 314.8 jit_solution(1739164244851850124)
XLA Ops:
  10.7 1.4 fusion.18
  13.6 8.2 %all-to-all-start = ((f32[16,256,2,4]{1,3,2,0:T(4,128)}), f32[16,256,2,4]{1,3,2,0:T(4,128)S(1)}, u32[]{:S(2)}, u32[]{:S(2)}) async-start(f32[16,256,2,4]{1,3,2,0:T(4,128)} %broadcast_in_dim.20), calls=%async_computation | async-start | bytes 262144 | tf_op jit(solution)/shard_map/all_to_all | solution.py:20
  21.9 7.8 %all-to-all-done = f32[16,256,2,4]{1,3,2,0:T(4,128)S(1)} async-done(((f32[16,256,2,4]{1,3,2,0:T(4,128)}), f32[16,256,2,4]{1,3,2,0:T(4,128)S(1)}, u32[]{:S(2)}, u32[]{:S(2)}) %all-to-all-start) | async-done | bytes 131104 | tf_op jit(solution)/shard_map/all_to_all | solution.py:20
  29.7 37.3 %all-gather.2.cloned.1.call-done = bf16[4096,4,128]{2,0,1:T(8,128)(2,1)} async-done(((bf16[256,4,128]{2,0,1:T(8,128)(2,1)}), bf16[4096,4,128]{2,0,1:T(8,128)(2,1)}) %all-gather.2.cloned.1.call-update) | async-done | bytes 4194320 | tf_op jit(solution)/shard_map/all_gather | solution.py:32
  67.0 3.8 %fusion.20 = (bf16[4096,2,128]{2,0,1:T(8,128)(2,1)S(1)}, bf16[4096,2,128]{2,0,1:T(8,128)(2,1)}) fusion(bf16[4096,4,128]{2,0,1:T(8,128)(2,1)} %all-gather.2.cloned.1.call-done), kind=kLoop, calls=%fused_computation.53 | loop fusion | bytes 8388608 | tf_op jit(solution)/shard_map/split | solution.py:33
  70.8 1.6 copy.73
  72.4 3.9 %copy.71 = bf16[16,256,2,128]{1,3,2,0:T(8,128)(2,1)} copy(bf16[16,256,2,128]{3,1,0,2:T(8,128)(2,1)} %bitcast.95) | data formatting | bytes 4194304
  76.4 2.4 broadcast_in_dim.18
  78.9 146.6 %while.16 = (s32[]{:T(128)}, f32[4096,2,128]{0,2,1:T(8,128)}, f32[256,2,128]{0,2,1:T(8,128)S(1)}, f32[256,2,128]{2,0,1:T(8,128)S(1)}, s32[16]{0:T(128)S(1)}, /*i...) while((s32[]{:T(128)}, f32[4096,2,128]{0,2,1:T(8,128)}, ...), condition=%wide.region_7.8_spmd.clone.clone, body=%wide.region_4.7_spmd.clone.clone.sunk | while | flops 170394112 | bytes 9207301 | solution.py:176
  80.1 7.9 %conditional.4 = ((f32[4096,2,128]{0,2,1:T(8,128)}, f32[256,2,128]{0,2,1:T(8,128)S(1)}, f32[256,2,128]{2,0,1:T(8,128)S(1)})) conditional(s32[]{:T(128)} %convert_element_type.92, (f32[4096,2,128]{0,2,1:T(8,128)}, f32[256,2,128]{0,2,1:T(8,128)S(1)}, f32[256,2,128]{2,0,1:T(8,128)S(1)}) %tuple.61, (s32[]{:T(128)}, f32[4096,2,128]{0,2,1:T(8,128)}, ...), branch_computations={%region_5.5_spmd, %region_6.6_spmd} | conditional | flops 170394112 | bytes 9205950 | solution.py:174
  83.2 1.3 fusion.5
  86.2 1.8 dynamic_update_slice.4
  89.3 7.9 %conditional.4 = ((f32[4096,2,128]{0,2,1:T(8,128)}, f32[256,2,128]{0,2,1:T(8,128)S(1)}, f32[256,2,128]{2,0,1:T(8,128)S(1)})) conditional(s32[]{:T(128)} %convert_element_type.92, (f32[4096,2,128]{0,2,1:T(8,128)}, f32[256,2,128]{0,2,1:T(8,128)S(1)}, f32[256,2,128]{2,0,1:T(8,128)S(1)}) %tuple.61, (s32[]{:T(128)}, f32[4096,2,128]{0,2,1:T(8,128)}, ...), branch_computations={%region_5.5_spmd, %region_6.6_spmd} | conditional | flops 170394112 | bytes 9205950 | solution.py:174
  92.4 1.3 fusion.5
  95.3 1.8 dynamic_update_slice.4
  98.4 7.9 %conditional.4 = ((f32[4096,2,128]{0,2,1:T(8,128)}, f32[256,2,128]{0,2,1:T(8,128)S(1)}, f32[256,2,128]{2,0,1:T(8,128)S(1)})) conditional(s32[]{:T(128)} %convert_element_type.92, (f32[4096,2,128]{0,2,1:T(8,128)}, f32[256,2,128]{0,2,1:T(8,128)S(1)}, f32[256,2,128]{2,0,1:T(8,128)S(1)}) %tuple.61, (s32[]{:T(128)}, f32[4096,2,128]{0,2,1:T(8,128)}, ...), branch_computations={%region_5.5_spmd, %region_6.6_spmd} | conditional | flops 170394112 | bytes 9205950 | solution.py:174
  101.5 1.3 fusion.5
  104.5 1.9 dynamic_update_slice.4
  107.6 8.0 %conditional.4 = ((f32[4096,2,128]{0,2,1:T(8,128)}, f32[256,2,128]{0,2,1:T(8,128)S(1)}, f32[256,2,128]{2,0,1:T(8,128)S(1)})) conditional(s32[]{:T(128)} %convert_element_type.92, (f32[4096,2,128]{0,2,1:T(8,128)}, f32[256,2,128]{0,2,1:T(8,128)S(1)}, f32[256,2,128]{2,0,1:T(8,128)S(1)}) %tuple.61, (s32[]{:T(128)}, f32[4096,2,128]{0,2,1:T(8,128)}, ...), branch_computations={%region_5.5_spmd, %region_6.6_spmd} | conditional | flops 170394112 | bytes 9205950 | solution.py:174
  110.7 1.3 fusion.5
  113.7 1.9 dynamic_update_slice.4
  116.8 7.9 %conditional.4 = ((f32[4096,2,128]{0,2,1:T(8,128)}, f32[256,2,128]{0,2,1:T(8,128)S(1)}, f32[256,2,128]{2,0,1:T(8,128)S(1)})) conditional(s32[]{:T(128)} %convert_element_type.92, (f32[4096,2,128]{0,2,1:T(8,128)}, f32[256,2,128]{0,2,1:T(8,128)S(1)}, f32[256,2,128]{2,0,1:T(8,128)S(1)}) %tuple.61, (s32[]{:T(128)}, f32[4096,2,128]{0,2,1:T(8,128)}, ...), branch_computations={%region_5.5_spmd, %region_6.6_spmd} | conditional | flops 170394112 | bytes 9205950 | solution.py:174
  119.9 1.3 fusion.5
  122.9 1.9 dynamic_update_slice.4
  126.0 7.9 %conditional.4 = ((f32[4096,2,128]{0,2,1:T(8,128)}, f32[256,2,128]{0,2,1:T(8,128)S(1)}, f32[256,2,128]{2,0,1:T(8,128)S(1)})) conditional(s32[]{:T(128)} %convert_element_type.92, (f32[4096,2,128]{0,2,1:T(8,128)}, f32[256,2,128]{0,2,1:T(8,128)S(1)}, f32[256,2,128]{2,0,1:T(8,128)S(1)}) %tuple.61, (s32[]{:T(128)}, f32[4096,2,128]{0,2,1:T(8,128)}, ...), branch_computations={%region_5.5_spmd, %region_6.6_spmd} | conditional | flops 170394112 | bytes 9205950 | solution.py:174
  129.1 1.3 fusion.5
  132.0 1.9 dynamic_update_slice.4
  135.2 7.9 %conditional.4 = ((f32[4096,2,128]{0,2,1:T(8,128)}, f32[256,2,128]{0,2,1:T(8,128)S(1)}, f32[256,2,128]{2,0,1:T(8,128)S(1)})) conditional(s32[]{:T(128)} %convert_element_type.92, (f32[4096,2,128]{0,2,1:T(8,128)}, f32[256,2,128]{0,2,1:T(8,128)S(1)}, f32[256,2,128]{2,0,1:T(8,128)S(1)}) %tuple.61, (s32[]{:T(128)}, f32[4096,2,128]{0,2,1:T(8,128)}, ...), branch_computations={%region_5.5_spmd, %region_6.6_spmd} | conditional | flops 170394112 | bytes 9205950 | solution.py:174
  138.3 1.3 fusion.5
  141.3 1.9 dynamic_update_slice.4
  144.4 7.9 %conditional.4 = ((f32[4096,2,128]{0,2,1:T(8,128)}, f32[256,2,128]{0,2,1:T(8,128)S(1)}, f32[256,2,128]{2,0,1:T(8,128)S(1)})) conditional(s32[]{:T(128)} %convert_element_type.92, (f32[4096,2,128]{0,2,1:T(8,128)}, f32[256,2,128]{0,2,1:T(8,128)S(1)}, f32[256,2,128]{2,0,1:T(8,128)S(1)}) %tuple.61, (s32[]{:T(128)}, f32[4096,2,128]{0,2,1:T(8,128)}, ...), branch_computations={%region_5.5_spmd, %region_6.6_spmd} | conditional | flops 170394112 | bytes 9205950 | solution.py:174
  147.4 1.3 fusion.5
  150.4 1.9 dynamic_update_slice.4
  153.6 7.9 %conditional.4 = ((f32[4096,2,128]{0,2,1:T(8,128)}, f32[256,2,128]{0,2,1:T(8,128)S(1)}, f32[256,2,128]{2,0,1:T(8,128)S(1)})) conditional(s32[]{:T(128)} %convert_element_type.92, (f32[4096,2,128]{0,2,1:T(8,128)}, f32[256,2,128]{0,2,1:T(8,128)S(1)}, f32[256,2,128]{2,0,1:T(8,128)S(1)}) %tuple.61, (s32[]{:T(128)}, f32[4096,2,128]{0,2,1:T(8,128)}, ...), branch_computations={%region_5.5_spmd, %region_6.6_spmd} | conditional | flops 170394112 | bytes 9205950 | solution.py:174
  156.6 1.3 fusion.5
  159.6 1.9 dynamic_update_slice.4
  162.8 7.9 %conditional.4 = ((f32[4096,2,128]{0,2,1:T(8,128)}, f32[256,2,128]{0,2,1:T(8,128)S(1)}, f32[256,2,128]{2,0,1:T(8,128)S(1)})) conditional(s32[]{:T(128)} %convert_element_type.92, (f32[4096,2,128]{0,2,1:T(8,128)}, f32[256,2,128]{0,2,1:T(8,128)S(1)}, f32[256,2,128]{2,0,1:T(8,128)S(1)}) %tuple.61, (s32[]{:T(128)}, f32[4096,2,128]{0,2,1:T(8,128)}, ...), branch_computations={%region_5.5_spmd, %region_6.6_spmd} | conditional | flops 170394112 | bytes 9205950 | solution.py:174
  165.8 1.3 fusion.5
  168.8 1.8 dynamic_update_slice.4
  171.9 7.9 %conditional.4 = ((f32[4096,2,128]{0,2,1:T(8,128)}, f32[256,2,128]{0,2,1:T(8,128)S(1)}, f32[256,2,128]{2,0,1:T(8,128)S(1)})) conditional(s32[]{:T(128)} %convert_element_type.92, (f32[4096,2,128]{0,2,1:T(8,128)}, f32[256,2,128]{0,2,1:T(8,128)S(1)}, f32[256,2,128]{2,0,1:T(8,128)S(1)}) %tuple.61, (s32[]{:T(128)}, f32[4096,2,128]{0,2,1:T(8,128)}, ...), branch_computations={%region_5.5_spmd, %region_6.6_spmd} | conditional | flops 170394112 | bytes 9205950 | solution.py:174
  175.0 1.3 fusion.5
  178.0 1.8 dynamic_update_slice.4
  181.1 7.9 %conditional.4 = ((f32[4096,2,128]{0,2,1:T(8,128)}, f32[256,2,128]{0,2,1:T(8,128)S(1)}, f32[256,2,128]{2,0,1:T(8,128)S(1)})) conditional(s32[]{:T(128)} %convert_element_type.92, (f32[4096,2,128]{0,2,1:T(8,128)}, f32[256,2,128]{0,2,1:T(8,128)S(1)}, f32[256,2,128]{2,0,1:T(8,128)S(1)}) %tuple.61, (s32[]{:T(128)}, f32[4096,2,128]{0,2,1:T(8,128)}, ...), branch_computations={%region_5.5_spmd, %region_6.6_spmd} | conditional | flops 170394112 | bytes 9205950 | solution.py:174
  184.1 1.3 fusion.5
  187.1 1.8 dynamic_update_slice.4
  190.2 7.9 %conditional.4 = ((f32[4096,2,128]{0,2,1:T(8,128)}, f32[256,2,128]{0,2,1:T(8,128)S(1)}, f32[256,2,128]{2,0,1:T(8,128)S(1)})) conditional(s32[]{:T(128)} %convert_element_type.92, (f32[4096,2,128]{0,2,1:T(8,128)}, f32[256,2,128]{0,2,1:T(8,128)S(1)}, f32[256,2,128]{2,0,1:T(8,128)S(1)}) %tuple.61, (s32[]{:T(128)}, f32[4096,2,128]{0,2,1:T(8,128)}, ...), branch_computations={%region_5.5_spmd, %region_6.6_spmd} | conditional | flops 170394112 | bytes 9205950 | solution.py:174
  193.3 1.3 fusion.5
  196.2 1.8 dynamic_update_slice.4
  199.3 7.9 %conditional.4 = ((f32[4096,2,128]{0,2,1:T(8,128)}, f32[256,2,128]{0,2,1:T(8,128)S(1)}, f32[256,2,128]{2,0,1:T(8,128)S(1)})) conditional(s32[]{:T(128)} %convert_element_type.92, (f32[4096,2,128]{0,2,1:T(8,128)}, f32[256,2,128]{0,2,1:T(8,128)S(1)}, f32[256,2,128]{2,0,1:T(8,128)S(1)}) %tuple.61, (s32[]{:T(128)}, f32[4096,2,128]{0,2,1:T(8,128)}, ...), branch_computations={%region_5.5_spmd, %region_6.6_spmd} | conditional | flops 170394112 | bytes 9205950 | solution.py:174
  202.4 1.3 fusion.5
  205.4 1.8 dynamic_update_slice.4
  208.5 7.9 %conditional.4 = ((f32[4096,2,128]{0,2,1:T(8,128)}, f32[256,2,128]{0,2,1:T(8,128)S(1)}, f32[256,2,128]{2,0,1:T(8,128)S(1)})) conditional(s32[]{:T(128)} %convert_element_type.92, (f32[4096,2,128]{0,2,1:T(8,128)}, f32[256,2,128]{0,2,1:T(8,128)S(1)}, f32[256,2,128]{2,0,1:T(8,128)S(1)}) %tuple.61, (s32[]{:T(128)}, f32[4096,2,128]{0,2,1:T(8,128)}, ...), branch_computations={%region_5.5_spmd, %region_6.6_spmd} | conditional | flops 170394112 | bytes 9205950 | solution.py:174
  211.6 1.3 fusion.5
  214.6 1.9 dynamic_update_slice.4
  217.7 7.8 %conditional.4 = ((f32[4096,2,128]{0,2,1:T(8,128)}, f32[256,2,128]{0,2,1:T(8,128)S(1)}, f32[256,2,128]{2,0,1:T(8,128)S(1)})) conditional(s32[]{:T(128)} %convert_element_type.92, (f32[4096,2,128]{0,2,1:T(8,128)}, f32[256,2,128]{0,2,1:T(8,128)S(1)}, f32[256,2,128]{2,0,1:T(8,128)S(1)}) %tuple.61, (s32[]{:T(128)}, f32[4096,2,128]{0,2,1:T(8,128)}, ...), branch_computations={%region_5.5_spmd, %region_6.6_spmd} | conditional | flops 170394112 | bytes 9205950 | solution.py:174
  223.7 1.8 dynamic_update_slice.4
  225.4 4.6 %copy.75 = bf16[4096,2,128]{2,0,1:T(8,128)(2,1)} copy(f32[4096,2,128]{0,2,1:T(8,128)} %get-tuple-element.177) | data formatting | bytes 6291456 | tf_op jit(solution)/shard_map/while | solution.py:176
  230.1 3.9 %copy.76 = bf16[16,256,2,128]{1,3,2,0:T(8,128)(2,1)} copy(bf16[16,256,2,128]{3,1,0,2:T(8,128)(2,1)} %bitcast.92) | data formatting | bytes 4194304 | tf_op jit(solution)/shard_map/reshape | solution.py:38
  234.0 32.9 %all_to_all.15 = bf16[16,256,2,128]{1,3,2,0:T(8,128)(2,1)} all-to-all(bf16[16,256,2,128]{1,3,2,0:T(8,128)(2,1)} %copy.76), channel_id=1, replica_groups=mesh['sp'=16,'tp'=8] {'sp'}, dimensions={0} | all-to-all | bytes 4194304 | tf_op jit(solution)/shard_map/all_to_all | solution.py:44
  267.0 1.9 reduce_sum.61
  269.6 1.5 copy.124
  271.1 4.4 %all-to-all-start.2 = ((bf16[16,256,256]{1,2,0:T(8,128)(2,1)}), bf16[16,256,256]{1,2,0:T(8,128)(2,1)}, u32[]{:S(2)}, u32[]{:S(2)}) async-start(bf16[16,256,256]{1,2,0:T(8,128)(2,1)} %bitcast.93), calls=%async_computation.2 | async-start | bytes 4194304 | tf_op jit(solution)/shard_map/all_to_all | solution.py:44
  278.0 27.3 %all-to-all-done.2 = bf16[16,256,256]{1,2,0:T(8,128)(2,1)} async-done(((bf16[16,256,256]{1,2,0:T(8,128)(2,1)}), bf16[16,256,256]{1,2,0:T(8,128)(2,1)}, u32[]{:S(2)}, u32[]{:S(2)}) %all-to-all-start.2) | async-done | bytes 2097184 | tf_op jit(solution)/shard_map/all_to_all | solution.py:44
  305.3 1.9 convert_reduce_fusion
  (273 shorter events, 94.9 us)
Async XLA Ops:
  7.2 261.7 %copy-start = (bf16[256,4096]{1,0:T(8,128)(2,1)S(1)}, bf16[256,4096]{1,0:T(8,128)(2,1)}, u32[]{:S(2)}) copy-start(bf16[256,4096]{1,0:T(8,128)(2,1)} %param.13) | copy-start | bytes 6291460
  7.2 5.7 %copy-start.4 = (f32[256,2,2]{0,2,1:T(2,128)S(1)}, f32[256,2,2]{0,2,1:T(2,128)}, u32[]{:S(2)}) copy-start(f32[256,2,2]{0,2,1:T(2,128)} %param.18) | copy-start | bytes 12292
  7.2 14.6 %copy-start.1 = (bf16[256,2,128]{2,1,0:T(2,128)(2,1)S(1)}, bf16[256,2,128]{2,1,0:T(2,128)(2,1)}, u32[]{:S(2)}) copy-start(bf16[256,2,128]{2,1,0:T(2,128)(2,1)} %param.15) | copy-start | bytes 393220
  7.2 14.7 %copy-start.2 = (bf16[256,2,128]{2,1,0:T(2,128)(2,1)S(1)}, bf16[256,2,128]{2,1,0:T(2,128)(2,1)}, u32[]{:S(2)}) copy-start(bf16[256,2,128]{2,1,0:T(2,128)(2,1)} %param.16) | copy-start | bytes 393220
  7.2 59.8 %all-gather.2.cloned.1.call-start = ((), (), s32[]{:S(2)}) async-start(), calls=%async_computation.3 | async-start | bytes 4456448 | tf_op jit(solution)/shard_map/all_gather | solution.py:32
  13.6 16.2 %all-to-all-start = ((f32[16,256,2,4]{1,3,2,0:T(4,128)}), f32[16,256,2,4]{1,3,2,0:T(4,128)S(1)}, u32[]{:S(2)}, u32[]{:S(2)}) async-start(f32[16,256,2,4]{1,3,2,0:T(4,128)} %broadcast_in_dim.20), calls=%async_computation | async-start | bytes 262144 | tf_op jit(solution)/shard_map/all_to_all | solution.py:20
  76.4 2.4 copy-start.3
  271.1 34.1 %all-to-all-start.2 = ((bf16[16,256,256]{1,2,0:T(8,128)(2,1)}), bf16[16,256,256]{1,2,0:T(8,128)(2,1)}, u32[]{:S(2)}, u32[]{:S(2)}) async-start(bf16[16,256,256]{1,2,0:T(8,128)(2,1)} %bitcast.93), calls=%async_computation.2 | async-start | bytes 4194304 | tf_op jit(solution)/shard_map/all_to_all | solution.py:44
Sparse Core Ops, SparseCore 0:
  13.0 53.9 all-gather.1
where the time goes:
time: 317 us; the launch traced here: 315 us
  local copies, waits for them, and re-layouts  85.9 us (27%)
  waiting for transfers between devices  72.3 us (23%)
  matrix products  56.5 us (18%)
  blocking collectives  32.9 us (10%)
  other arithmetic  28.1 us (9%)
  between operations  14.2 us (4%)
  starting transfers between devices  12.6 us (4%)
  loops' own time  12.2 us (4%)
    all_gather x1, waiting for transfers between devices, side_by_side(): result = lax.all_gather(both, axis, axis=dim, tiled=True)  37.3 us
    all_to_all x1, blocking collectives, sent_and_summed(): lax.all_to_all(blocks, axis, split_axis=0, concat_axis=0, tiled=True)  32.9 us
    dynamic_update_slice x16, local copies, waits for them, and re-layouts, add_rows(): lax.dynamic_update_slice_in_dim(buffer, current + addition, anchor, 0)  29.6 us
    all_to_all x1, waiting for transfers between devices, sent_and_summed(): lax.all_to_all(blocks, axis, split_axis=0, concat_axis=0, tiled=True)  27.3 us
    dynamic_slice x32, local copies, waits for them, and re-layouts, body(): result, _ = lax.scan(visit, (global_zero, local_zero, local_zero), blocks)  24 us
    dot_general x16, matrix products, block_grads(): jnp.einsum('hqk,qhe->khe', diff_weights, grad_blk, preferred_element_type...  20.3 us
    add x16, other arithmetic, accumulate(): key_acc + key_part  19.2 us
    dot_general x16, matrix products, block_grads(): jnp.einsum('qhe,khe->hqk', grad_blk, value_blk, preferred_element_type=jn...  18.1 us
  transfers between devices with their start and end apart: 3, of which 3 were waited for; matrix products, arithmetic and copies ran while one was open for 1% of the time, Pallas kernels for 0%

commit v1 on v0

v1 whole, which is shorter than its diff:
```python
import functools

import jax
import jax.numpy as jnp
from jax import lax
from jax.experimental import pallas as pl
from jax.experimental.pallas import tpu as pltpu
from jax.sharding import PartitionSpec as P

F32 = jnp.float32
BF16 = jnp.bfloat16
EPSILON = 1e-05
LOG2E = 1.4426950408889634
SCALE = 0.125
T = 256
W = 128
NT = (((1,), (1,)), ((), ()))


def dot(a, b):
    return jnp.dot(a, b, preferred_element_type=F32)


def dot_nt(a, b):
    return lax.dot_general(a, b, NT, preferred_element_type=F32)


def kernel(
    q_ref, k_ref, v_ref, mo_ref, lse_ref, og_ref, lam_ref, gain_ref, lat_hbm,
    qg_ref, kg_ref, vg_ref, wg_ref,
    lat, qdo, kv, st, dqt, dkv, wide, wide2, dqf,
    qtx, qrx, ktx, krx, atx, arx, btx, brx,
    lat_sem, gs, gr, rs, rr,
):
    sp = lax.axis_index("sp")
    tp = lax.axis_index("tp")
    z = sp // 4
    y = sp % 4
    pos = (y, z)

    def ring(axis, step):
        moved = lax.rem(pos[axis] + step + 4, 4)
        return moved

    def peer(axis, step):
        moved = ring(axis, step)
        return (z * 4 + moved if axis == 0 else moved * 4 + y, tp)

    def remote(src, dst, send, recv, device):
        return pltpu.make_async_remote_copy(
            src_ref=src, dst_ref=dst, send_sem=send, recv_sem=recv,
            device_id=device, device_id_type=pl.DeviceIdType.MESH,
        )

    barrier = pltpu.get_barrier_semaphore()
    for axis in (0, 1):
        for step in (1, -1):
            pl.semaphore_signal(
                barrier, inc=1, device_id=peer(axis, step), device_id_type=pl.DeviceIdType.MESH
            )
    lat_copy = pltpu.make_async_copy(lat_hbm, lat, lat_sem)
    lat_copy.start()

    qpos = (y, z)
    kpos = (z, y)
    wide[0] = q_ref[...].astype(F32)
    wide[1] = k_ref[...].astype(F32)
    wide[2] = v_ref[...].astype(F32)
    wide[3] = og_ref[...].astype(F32)
    for h in (0, 1):
        qdo[h, qpos[h], 0] = wide[0, pl.ds(h, T, stride=2), :].astype(BF16)
        kv[h, kpos[h], 0] = wide[1, pl.ds(h, T, stride=2), :].astype(BF16)
        kv[h, kpos[h], 1] = wide[2, pl.ds(h, T, stride=2), :].astype(BF16)
    pl.semaphore_wait(barrier, 4)

    qh = (0, 1)
    kh = (1, 0)
    first = {}

    def item(axis, name, slot):
        if name == "q":
            return qdo.at[qh[axis], slot, 0]
        if name == "do":
            return qdo.at[qh[axis], slot, 1]
        if name == "st":
            return st.at[qh[axis], slot]
        if name == "k":
            return kv.at[kh[axis], slot, 0]
        return kv.at[kh[axis], slot, 1]

    names = ("q", "k", "v", "do", "st")

    def send_own(some):
        for name in some:
            for axis in (0, 1):
                for d, step in enumerate((1, -1)):
                    n = names.index(name)
                    ref = item(axis, name, pos[axis])
                    c = remote(ref, ref, gs.at[axis, d, n], gr.at[axis, d, n], peer(axis, step))
                    c.start()
                    first[axis, d, name] = c

    send_own(("q", "k", "v"))

    wide2[...] = mo_ref[...].astype(F32)
    gain = gain_ref[...]
    for h in (0, 1):
        lam = lam_ref[h]
        m1 = wide2[pl.ds(h, T, stride=4), :]
        m2 = wide2[pl.ds(2 + h, T, stride=4), :]
        comb = m1 - lam * m2
        inv = lax.rsqrt(jnp.mean(comb * comb, axis=-1, keepdims=True) + EPSILON)
        wtd = gain * wide[3, pl.ds(h, T, stride=2), :]
        cross = jnp.mean(comb * wtd, axis=-1, keepdims=True)
        grad = (inv * wtd - inv * inv * inv * comb * cross).astype(BF16)
        qdo[h, qpos[h], 1] = grad
        gf = grad.astype(F32)
        r1 = jnp.sum(jnp.transpose(gf * m1), axis=0, keepdims=True)
        r2 = jnp.sum(jnp.transpose(gf * m2), axis=0, keepdims=True)
        lam_row = jnp.full((1, T), lam, F32)
        st[h, qpos[h], 0:1] = lse_ref[2 * h : 2 * h + 1, :] * LOG2E
        st[h, qpos[h], 1:2] = (lse_ref[2 * h + 1 : 2 * h + 2, :] - jnp.log(lam_row)) * LOG2E
        st[h, qpos[h], 2:3] = r1
        st[h, qpos[h], 3:4] = r2
        st[h, qpos[h], 4:8] = jnp.zeros((4, T), F32)
    send_own(("do", "st"))

    dqt[...] = jnp.zeros_like(dqt)
    dkv[...] = jnp.zeros_like(dkv)

    lane = lax.broadcasted_iota(jnp.int32, (T, W), 1)

    def unit(h, qs, ks, masked):
        q = qdo[h, qs, 0]
        do = qdo[h, qs, 1]
        k = kv[h, ks, 0]
        v = kv[h, ks, 1]
        zero = jnp.zeros_like(q)
        q1 = jnp.where(lane < 64, q, zero)
        q2 = jnp.where(lane < 64, zero, -q)
        s1 = dot_nt(k, q1)
        s2 = dot_nt(k, q2)
        dp = dot_nt(v, do)
        p1 = jnp.exp2(s1 * (SCALE * LOG2E) - st[h, qs, 0:1])
        p2 = jnp.exp2(s2 * (-SCALE * LOG2E) - st[h, qs, 1:2])
        if masked:
            rows = lax.broadcasted_iota(jnp.int32, (T, T), 0)
            cols = lax.broadcasted_iota(jnp.int32, (T, T), 1)
            keep = rows <= cols
            p1 = jnp.where(keep, p1, 0.0)
            p2 = jnp.where(keep, p2, 0.0)
        w = (p1 - p2).astype(BF16)
        d1 = (p1 * (dp - st[h, qs, 2:3])).astype(BF16)
        d2 = (p2 * (dp - st[h, qs, 3:4])).astype(BF16)
        kt = jnp.transpose(k)
        dqt[h, qs, 0:64] += dot(kt[0:64], d1)
        dqt[h, qs, 64:128] -= dot(kt[64:128], d2)
        dkv[h, ks, 0] += dot(d1, q1) + dot(d2, q2)
        dkv[h, ks, 1] += dot(w, do)

    unit(0, y, z, True)
    unit(1, z, y, True)

    second = []
    for axis in (0, 1):
        for d, some in ((0, ("q", "k")), (1, ("do", "v", "st"))):
            for name in some:
                first[axis, d, name].wait_recv()
                step = 1 if d == 0 else -1
                ref = item(axis, name, ring(axis, -step))
                n = 5 + names.index(name)
                c = remote(ref, ref, gs.at[axis, d, n], gr.at[axis, d, n], peer(axis, step))
                c.start()
                second.append(c)
    for axis in (0, 1):
        for d, some in ((1, ("q", "k")), (0, ("do", "v", "st"))):
            for name in some:
                first[axis, d, name].wait_recv()
    for c in second:
        c.wait_recv()

    count_a = 4 * z + 3 - y

    def step_unit(n, carry):
        i = n + jnp.where(n >= 4 * z, y + 1, 0)
        u = n - count_a
        w = u - y
        in_a = n < count_a
        h = jnp.where(in_a, 0, 1)
        near = u < y
        qs = jnp.where(in_a, i % 4, jnp.where(near, z, z + 1 + w // 4))
        ks = jnp.where(in_a, i // 4, jnp.where(near, u, (w + 4) % 4))
        unit(h, qs, ks, False)
        return carry

    lax.fori_loop(0, 15, step_unit, 0)

    def reduce_start(tx, rx, axis, base, get):
        out = []

        def go(j, value, step):
            tx[axis, j] = value.astype(BF16)
            c = remote(
                tx.at[axis, j], rx.at[axis, j], rs.at[axis, base + j], rr.at[axis, base + j],
                peer(axis, step),
            )
            c.start()
            out.append(c)

        far, up, down = ring(axis, 2), ring(axis, 1), ring(axis, -1)
        go(0, get(far, 0), 1)
        go(1, get(far, 1), -1)
        go(2, get(up, 1), 1)
        go(3, get(down, 0), -1)
        return (out, go)

    def reduce_middle(state, tx, rx, axis, get):
        out, go = state
        up, down = ring(axis, 1), ring(axis, -1)
        mine = get(up, 0)
        out[0].wait_recv()
        go(4, mine + rx[axis, 0].astype(F32), 1)
        mine = get(down, 1)
        out[1].wait_recv()
        go(5, mine + rx[axis, 1].astype(F32), -1)

    def reduce_end(state, rx, axis, get):
        out, _ = state
        own0 = get(pos[axis], 0)
        own1 = get(pos[axis], 1)
        for j in (2, 3, 4, 5):
            out[j].wait_recv()
        r0 = own0 + rx[axis, 3].astype(F32) + rx[axis, 4].astype(F32)
        r1 = own1 + rx[axis, 2].astype(F32) + rx[axis, 5].astype(F32)
        return r0, r1

    def get_dq(h):
        return lambda slot, p: dqt[h, slot, 64 * p : 64 * p + 64] * SCALE

    def get_dkv(h):
        return lambda slot, p: dkv[h, slot, p] * (SCALE if p == 0 else 1.0)

    dq_state = {}
    for h in (0, 1):
        dq_state[h] = reduce_start(qtx, qrx, h, 0, get_dq(h))
    for h in (0, 1):
        reduce_middle(dq_state[h], qtx, qrx, h, get_dq(h))
    lat_copy.wait()

    def block_a(z_to, y_to):
        return z_to * 4 + y_to

    def get_wg(h):
        def get(slot, p):
            parts = []
            for o in (2 * p, 2 * p + 1):
                blk = block_a(o, slot) if h == 0 else block_a(slot, o)
                cols = lat[:, pl.ds(pl.multiple_of(blk * T, T), T)]
                parts.append(dot(dqf[h], cols))
            return jnp.stack(parts)

        return get

    a_state = {}
    for h in (0, 1):
        r0, r1 = reduce_end(dq_state[h], qrx, h, get_dq(h))
        dqf[h, 0:64] = r0.astype(BF16)
        dqf[h, 64:128] = r1.astype(BF16)
        a_state[h] = reduce_start(atx, arx, h, 6, get_wg(h))

    k_state = {}
    for axis in (0, 1):
        k_state[axis] = reduce_start(ktx, krx, axis, 18, get_dkv(1 - axis))
    for h in (0, 1):
        wide[0, pl.ds(h, T, stride=2), :] = jnp.transpose(dqf[h].astype(F32))
    qg_ref[...] = wide[0].astype(BF16)
    for h in (0, 1):
        reduce_middle(a_state[h], atx, arx, h, get_wg(h))
    for axis in (0, 1):
        reduce_middle(k_state[axis], ktx, krx, axis, get_dkv(1 - axis))
    b_state = {}
    b_get = {}
    for h in (0, 1):
        r0, r1 = reduce_end(a_state[h], arx, h, get_wg(h))
        wide_b = wide2
        for o in range(4):
            part = r0[o] if o < 2 else r1[o - 2]
            wide_b[pl.ds(o * 128, 128), :] = part[:, 0:128] if h == 0 else part[:, 0:128]
            wide_b[pl.ds(512 + o * 128, 128), :] = part[:, 128:256]

        def get(slot, p):
            start = pl.multiple_of(slot * 128 + 64 * p, 64)
            return jnp.concatenate(
                [wide2[pl.ds(start, 64), :], wide2[pl.ds(start + 512, 64), :]], axis=1
            )

        other = 1 - h
        own = (get(pos[other], 0), get(pos[other], 1))
        ups = (get(ring(other, 1), 0), get(ring(other, -1), 1))
        b_state[h] = reduce_start(btx, brx, other, 12, get)
        b_get[h] = (own, ups)
    for h in (0, 1):
        own, ups = b_get[h]
        other = 1 - h
        out, go = b_state[h]
        out[0].wait_recv()
        go(4, ups[0] + brx[other, 0].astype(F32), 1)
        out[1].wait_recv()
        go(5, ups[1] + brx[other, 1].astype(F32), -1)
    for axis in (0, 1):
        h = 1 - axis
        r0, r1 = reduce_end(k_state[axis], krx, axis, get_dkv(h))
        wide[1, pl.ds(h, T, stride=2), :] = r0
        wide[2, pl.ds(h, T, stride=2), :] = r1
    kg_ref[...] = wide[1].astype(BF16)
    vg_ref[...] = wide[2].astype(BF16)
    for h in (0, 1):
        own, _ = b_get[h]
        other = 1 - h
        r0, r1 = reduce_end(b_state[h], brx, other, lambda slot, p: own[p])
        wg_ref[:, h * W : h * W + W] = jnp.transpose(jnp.concatenate([r0, r1], axis=0))

    for c in first.values():
        c.wait_send()
    for c in second:
        c.wait_send()
    for states in (dq_state, a_state, k_state, b_state):
        for out, _ in states.values():
            for c in out:
                c.wait_send()


def body(latents, query_heads, key_heads, value_heads, map_outputs, log_sums, out_grad, mix_lambda, norm_gain):
    rows = 2 * T
    vmem = pl.BlockSpec(memory_space=pltpu.VMEM)
    outs = pl.pallas_call(
        kernel,
        out_shape=(
            jax.ShapeDtypeStruct((rows, W), BF16),
            jax.ShapeDtypeStruct((rows, W), BF16),
            jax.ShapeDtypeStruct((rows, W), BF16),
            jax.ShapeDtypeStruct((T, 2 * W), F32),
        ),
        in_specs=[
            vmem, vmem, vmem, vmem, vmem, vmem,
            pl.BlockSpec(memory_space=pltpu.SMEM), vmem,
            pl.BlockSpec(memory_space=pl.ANY),
        ],
        out_specs=(vmem, vmem, vmem, vmem),
        scratch_shapes=[
            pltpu.VMEM((T, 4096), BF16),
            pltpu.VMEM((2, 4, 2, T, W), BF16),
            pltpu.VMEM((2, 4, 2, T, W), BF16),
            pltpu.VMEM((2, 4, 8, T), F32),
            pltpu.VMEM((2, 4, W, T), F32),
            pltpu.VMEM((2, 4, 2, T, W), F32),
            pltpu.VMEM((4, rows, W), F32),
            pltpu.VMEM((4 * T, W), F32),
            pltpu.VMEM((2, W, T), BF16),
            pltpu.VMEM((2, 6, 64, T), BF16),
            pltpu.VMEM((2, 6, 64, T), BF16),
            pltpu.VMEM((2, 6, T, W), BF16),
            pltpu.VMEM((2, 6, T, W), BF16),
            pltpu.VMEM((2, 6, 2, W, T), BF16),
            pltpu.VMEM((2, 6, 2, W, T), BF16),
            pltpu.VMEM((2, 6, 64, T), BF16),
            pltpu.VMEM((2, 6, 64, T), BF16),
            pltpu.SemaphoreType.DMA,
            pltpu.SemaphoreType.DMA((2, 2, 10)),
            pltpu.SemaphoreType.DMA((2, 2, 10)),
            pltpu.SemaphoreType.DMA((2, 24)),
            pltpu.SemaphoreType.DMA((2, 24)),
        ],
        compiler_params=pltpu.CompilerParams(
            collective_id=0, has_side_effects=True, vmem_limit_bytes=48 * 1024 * 1024
        ),
    )(
        query_heads.reshape(rows, W),
        key_heads.reshape(rows, W),
        value_heads.reshape(rows, W),
        map_outputs.reshape(2 * rows, W),
        jnp.transpose(log_sums, (1, 2, 0)).reshape(4, T),
        out_grad.reshape(rows, W),
        mix_lambda,
        norm_gain.reshape(1, W),
        latents,
    )
    qg, kg, vg, wg = outs
    shape = query_heads.shape
    return (qg.reshape(shape), kg.reshape(shape), vg.reshape(shape), wg)


def solution(mesh):
    placed = (
        P("sp", None),
        P("sp", "tp", None),
        P("sp", "tp", None),
        P("sp", "tp", None),
        P("sp", None, "tp", None),
        P("sp", "tp", None),
        P("sp", "tp", None),
        P("tp"),
        P(),
    )
    return jax.shard_map(
        body,
        mesh=mesh,
        in_specs=placed,
        out_specs=(P("sp", "tp", None), P("sp", "tp", None), P("sp", "tp", None), P("sp", "tp")),
        check_vma=False,
    )
```

time: 317 us -> 67.1 us (0.21)
  local copies, waits for them, and re-layouts: 85.9 us -> 10.8 us
  waiting for transfers between devices: 72.3 us -> 0 us
  matrix products: 56.5 us -> 0 us
  Pallas kernels: 0 us -> 55.3 us
  blocking collectives: 32.9 us -> 0 us
  other arithmetic: 28.1 us -> 0 us
  between operations: 14.2 us -> 0.65 us
  starting transfers between devices: 12.6 us -> 0 us
  loops' own time: 12.2 us -> 0 us
    dot_general x81 -> x0, matrix products: 56.5 us -> none  [the longest x16 20.3 us: block_grads(): jnp.einsum('hqk,qhe->khe', diff_weights, grad_blk, preferred_element_type...]
    pallas_call x0 -> x1, Pallas kernels: none -> 55.3 us  [body(): pl.pallas_call(kernel, out_shape=(jax.ShapeDtypeStruct((rows, W), BF16),...]
    all_gather x1 -> x0, waiting for transfers between devices: 37.3 us -> none  [side_by_side(): result = lax.all_gather(both, axis, axis=dim, tiled=True)]
    all_to_all x2 -> x0, waiting for transfers between devices: 35.1 us -> none  [the longest x1 27.3 us: sent_and_summed(): lax.all_to_all(blocks, axis, split_axis=0, concat_axis=0, tiled=True)]
    all_to_all x1 -> x0, blocking collectives: 32.9 us -> none  [sent_and_summed(): lax.all_to_all(blocks, axis, split_axis=0, concat_axis=0, tiled=True)]
    dynamic_update_slice x16 -> x0, local copies, waits for them, and re-layouts: 29.6 us -> none  [add_rows(): lax.dynamic_update_slice_in_dim(buffer, current + addition, anchor, 0)]
    dynamic_slice x32 -> x0, local copies, waits for them, and re-layouts: 24 us -> none  [body(): result, _ = lax.scan(visit, (global_zero, local_zero, local_zero), blocks)]
    add x48 -> x0, other arithmetic: 19.3 us -> none  [the longest x16 19.2 us: accumulate(): key_acc + key_part]
  transfers between devices with their start and end apart: 3 -> 0, of which waited for: 3 -> 0; matrix products, arithmetic and copies ran while one was open for 1% -> 0% of each run, Pallas kernels for 0% -> 0%
where the time goes in v1:
time: 67.1 us; the launch traced here: 66.8 us
  Pallas kernels  55.3 us (82%)
  local copies, waits for them, and re-layouts  10.8 us (16%)
    pallas_call x1, Pallas kernels, body(): pl.pallas_call(kernel, out_shape=(jax.ShapeDtypeStruct((rows, W), BF16),...  55.3 us
    unnamed x20, local copies, waits for them, and re-layouts  10.1 us

profile of v1, /device:TPU:0, one launch (start us, length us, event | category | flops | bytes accessed | tf_op | source)
XLA Modules:
  0.0 66.8 jit_solution(3850259444798219180)
XLA Ops:
  0.6 0.7 %reshape.42.lse_ref = f32[4,256]{1,0:T(4,128)S(1)} reshape(f32[2,2,256]{2,1,0:T(2,128)} %bitcast.19) | data formatting | bytes 8192 | tf_op jit(solution)/shard_map/reshape | solution.py:382
  1.3 0.0 copy-start
  1.3 1.6 %copy-done = bf16[256,4096]{1,0:T(8,128)(2,1)S(1)} copy-done((bf16[256,4096]{1,0:T(8,128)(2,1)S(1)}, bf16[256,4096]{1,0:T(8,128)(2,1)}, u32[]{:S(2)}) %copy-start) | copy-done | bytes 2097176
  2.9 0.0 copy-start.1
  2.9 0.9 %copy-done.1 = bf16[256,2,2,128]{3,2,1,0:T(2,128)(2,1)S(1)} copy-done((bf16[256,2,2,128]{3,2,1,0:T(2,128)(2,1)S(1)}, bf16[256,2,2,128]{3,2,1,0:T(2,128)(2,1)}, u32[]{:S(2)}) %copy-start.1) | copy-done | bytes 262168
  3.9 0.0 copy-start.2
  3.9 0.9 %copy-done.2 = bf16[256,2,128]{2,1,0:T(2,128)(2,1)S(1)} copy-done((bf16[256,2,128]{2,1,0:T(2,128)(2,1)S(1)}, bf16[256,2,128]{2,1,0:T(2,128)(2,1)}, u32[]{:S(2)}) %copy-start.2) | copy-done | bytes 131096
  4.8 0.0 copy-start.3
  4.8 0.9 %copy-done.3 = bf16[256,2,128]{2,1,0:T(2,128)(2,1)S(1)} copy-done((bf16[256,2,128]{2,1,0:T(2,128)(2,1)S(1)}, bf16[256,2,128]{2,1,0:T(2,128)(2,1)}, u32[]{:S(2)}) %copy-start.3) | copy-done | bytes 131096
  5.7 0.0 copy-start.4
  5.7 0.9 %copy-done.4 = bf16[256,2,128]{2,1,0:T(2,128)(2,1)S(1)} copy-done((bf16[256,2,128]{2,1,0:T(2,128)(2,1)S(1)}, bf16[256,2,128]{2,1,0:T(2,128)(2,1)}, u32[]{:S(2)}) %copy-start.4) | copy-done | bytes 131096
  6.6 0.0 copy-start.5
  6.6 0.9 %copy-done.5 = bf16[256,2,128]{2,1,0:T(2,128)(2,1)S(1)} copy-done((bf16[256,2,128]{2,1,0:T(2,128)(2,1)S(1)}, bf16[256,2,128]{2,1,0:T(2,128)(2,1)}, u32[]{:S(2)}) %copy-start.5) | copy-done | bytes 131096
  7.5 0.0 copy-start.6
  7.5 0.7 copy-done.6
  8.1 0.0 copy-start.7
  8.2 0.7 copy-done.7
  8.8 55.3 %shard_map.120 = (bf16[512,128]{1,0:T(8,128)(2,1)S(1)}, bf16[512,128]{1,0:T(8,128)(2,1)S(1)}, bf16[512,128]{1,0:T(8,128)(2,1)S(1)}, f32[256,256]{1,0:T(8,128)S(1)}) custom-call(bf16[512,128]{1,0:T(8,128)(2,1)S(1)} %bitcast.14, bf16[512,128]{1,0:T(8,128)(2,1)S(1)} %bitcast.15, bf16[512,128]{1,0:T(8,128)(2,1)S(1)} %bitcast.16, bf16[1024,128]{1,0:T(8,128)(2,1)S(1)} %bitcast.10, ...), custom_call_target="tpu_custom_call" | custom-call | tf_op jit(solution)/shard_map/pallas_call | solution.py:336
  64.1 0.7 copy.17
  64.8 0.7 copy.18
  65.4 0.7 copy.19
  66.1 0.7 %copy.20 = f32[256,256]{1,0:T(8,128)} copy(f32[256,256]{1,0:T(8,128)S(1)} %get-tuple-element.19) | data formatting | bytes 524288
Async XLA Ops:
  1.3 1.6 %copy-start = (bf16[256,4096]{1,0:T(8,128)(2,1)S(1)}, bf16[256,4096]{1,0:T(8,128)(2,1)}, u32[]{:S(2)}) copy-start(bf16[256,4096]{1,0:T(8,128)(2,1)} %lat_hbm.1) | copy-start | bytes 6291460
  2.9 0.9 %copy-start.1 = (bf16[256,2,2,128]{3,2,1,0:T(2,128)(2,1)S(1)}, bf16[256,2,2,128]{3,2,1,0:T(2,128)(2,1)}, u32[]{:S(2)}) copy-start(bf16[256,2,2,128]{3,2,1,0:T(2,128)(2,1)} %param.13) | copy-start | bytes 786436
  3.9 0.9 %copy-start.2 = (bf16[256,2,128]{2,1,0:T(2,128)(2,1)S(1)}, bf16[256,2,128]{2,1,0:T(2,128)(2,1)}, u32[]{:S(2)}) copy-start(bf16[256,2,128]{2,1,0:T(2,128)(2,1)} %param.10) | copy-start | bytes 393220
  4.8 0.9 %copy-start.3 = (bf16[256,2,128]{2,1,0:T(2,128)(2,1)S(1)}, bf16[256,2,128]{2,1,0:T(2,128)(2,1)}, u32[]{:S(2)}) copy-start(bf16[256,2,128]{2,1,0:T(2,128)(2,1)} %param.11) | copy-start | bytes 393220
  5.7 0.9 %copy-start.4 = (bf16[256,2,128]{2,1,0:T(2,128)(2,1)S(1)}, bf16[256,2,128]{2,1,0:T(2,128)(2,1)}, u32[]{:S(2)}) copy-start(bf16[256,2,128]{2,1,0:T(2,128)(2,1)} %param.12) | copy-start | bytes 393220
  6.6 0.9 %copy-start.5 = (bf16[256,2,128]{2,1,0:T(2,128)(2,1)S(1)}, bf16[256,2,128]{2,1,0:T(2,128)(2,1)}, u32[]{:S(2)}) copy-start(bf16[256,2,128]{2,1,0:T(2,128)(2,1)} %param.15) | copy-start | bytes 393220
  7.5 0.7 copy-start.6
  8.1 0.7 copy-start.7

commit v2 on v1

v2 whole, which is shorter than its diff:
```python
import functools

import jax
import jax.numpy as jnp
from jax import lax
from jax.experimental import pallas as pl
from jax.experimental.pallas import tpu as pltpu
from jax.sharding import PartitionSpec as P

F32 = jnp.float32
BF16 = jnp.bfloat16
EPSILON = 1e-05
LOG2E = 1.4426950408889634
SCALE = 0.125
T = 256
W = 128
VMEM_ALL = 67043328
NT = (((1,), (1,)), ((), ()))


def dot(a, b):
    return jnp.dot(a, b, preferred_element_type=F32)


def dot_nt(a, b):
    return lax.dot_general(a, b, NT, preferred_element_type=F32)


def kernel(
    q_hbm, k_hbm, v_hbm, mo_hbm, lse_hbm, og_hbm, lam_hbm, gain_hbm, lat_hbm,
    qg_hbm, kg_hbm, vg_hbm, wg_hbm,
    q_in, k_in, v_in, mo_in, lse_in, og_in, lam_in, gain_in,
    lat, qdo, kv, st, dqt, dkv, wide, wide2, dqf,
    qtx, qrx, ktx, krx, atx, arx, btx, brx,
    qg_ref, kg_ref, vg_ref, wg_ref,
    in_sem, out_sem, gs, gr, rs, rr,
):
    sp = lax.axis_index("sp")
    tp = lax.axis_index("tp")
    z = sp // 4
    y = sp % 4
    pos = (y, z)

    def ring(axis, step):
        return lax.rem(pos[axis] + step + 4, 4)

    def peer(axis, step):
        moved = ring(axis, step)
        return (z * 4 + moved if axis == 0 else moved * 4 + y, tp)

    def remote(src, dst, send, recv, device):
        return pltpu.make_async_remote_copy(
            src_ref=src, dst_ref=dst, send_sem=send, recv_sem=recv,
            device_id=device, device_id_type=pl.DeviceIdType.MESH,
        )

    barrier = pltpu.get_barrier_semaphore()
    for axis in (0, 1):
        for step in (1, -1):
            pl.semaphore_signal(
                barrier, inc=1, device_id=peer(axis, step), device_id_type=pl.DeviceIdType.MESH
            )
    sources = (q_hbm, k_hbm, v_hbm, og_hbm, mo_hbm, lse_hbm, lam_hbm, gain_hbm, lat_hbm)
    targets = (q_in, k_in, v_in, og_in, mo_in, lse_in, lam_in, gain_in, lat)
    loads = [pltpu.make_async_copy(a, b, in_sem.at[n]) for n, (a, b) in enumerate(zip(sources, targets))]
    for c in loads:
        c.start()

    qpos = (y, z)
    kpos = (z, y)
    for n, ref in enumerate((q_in, k_in, v_in)):
        loads[n].wait()
        wide[n] = ref[...].astype(F32)
    for h in (0, 1):
        qdo[h, qpos[h], 0] = wide[0, pl.ds(h, T, stride=2), :].astype(BF16)
        kv[h, kpos[h], 0] = wide[1, pl.ds(h, T, stride=2), :].astype(BF16)
        kv[h, kpos[h], 1] = wide[2, pl.ds(h, T, stride=2), :].astype(BF16)
    pl.semaphore_wait(barrier, 4)

    qh = (0, 1)
    kh = (1, 0)
    first = {}

    def item(axis, name, slot):
        if name == "q":
            return qdo.at[qh[axis], slot, 0]
        if name == "do":
            return qdo.at[qh[axis], slot, 1]
        if name == "st":
            return st.at[qh[axis], slot]
        if name == "k":
            return kv.at[kh[axis], slot, 0]
        return kv.at[kh[axis], slot, 1]

    names = ("q", "k", "v", "do", "st")

    def send_own(some):
        for name in some:
            for axis in (0, 1):
                for d, step in enumerate((1, -1)):
                    n = names.index(name)
                    ref = item(axis, name, pos[axis])
                    c = remote(ref, ref, gs.at[axis, d, n], gr.at[axis, d, n], peer(axis, step))
                    c.start()
                    first[axis, d, name] = c

    send_own(("q", "k", "v"))

    for c in loads[3:8]:
        c.wait()
    wide[3] = og_in[...].astype(F32)
    wide2[...] = mo_in[...].astype(F32)
    gain = gain_in[...]
    for h in (0, 1):
        lam = lam_in[h]
        m1 = wide2[pl.ds(h, T, stride=4), :]
        m2 = wide2[pl.ds(2 + h, T, stride=4), :]
        comb = m1 - lam * m2
        inv = lax.rsqrt(jnp.mean(comb * comb, axis=-1, keepdims=True) + EPSILON)
        wtd = gain * wide[3, pl.ds(h, T, stride=2), :]
        cross = jnp.mean(comb * wtd, axis=-1, keepdims=True)
        grad = (inv * wtd - inv * inv * inv * comb * cross).astype(BF16)
        qdo[h, qpos[h], 1] = grad
        gf = grad.astype(F32)
        r1 = jnp.sum(jnp.transpose(gf * m1), axis=0, keepdims=True)
        r2 = jnp.sum(jnp.transpose(gf * m2), axis=0, keepdims=True)
        lam_row = jnp.full((1, T), lam, F32)
        st[h, qpos[h], 0:1] = lse_in[h, 0:1, :] * LOG2E
        st[h, qpos[h], 1:2] = (lse_in[h, 1:2, :] - jnp.log(lam_row)) * LOG2E
        st[h, qpos[h], 2:3] = r1
        st[h, qpos[h], 3:4] = r2
        st[h, qpos[h], 4:8] = jnp.zeros((4, T), F32)
    send_own(("do", "st"))

    dqt[...] = jnp.zeros_like(dqt)
    dkv[...] = jnp.zeros_like(dkv)

    lane = lax.broadcasted_iota(jnp.int32, (T, W), 1)

    def unit(h, qs, ks, masked):
        q = qdo[h, qs, 0]
        do = qdo[h, qs, 1]
        k = kv[h, ks, 0]
        v = kv[h, ks, 1]
        zero = jnp.zeros_like(q)
        q1 = jnp.where(lane < 64, q, zero)
        q2 = jnp.where(lane < 64, zero, -q)
        s1 = dot_nt(k, q1)
        s2 = dot_nt(k, q2)
        dp = dot_nt(v, do)
        p1 = jnp.exp2(s1 * (SCALE * LOG2E) - st[h, qs, 0:1])
        p2 = jnp.exp2(s2 * (-SCALE * LOG2E) - st[h, qs, 1:2])
        if masked:
            rows = lax.broadcasted_iota(jnp.int32, (T, T), 0)
            cols = lax.broadcasted_iota(jnp.int32, (T, T), 1)
            keep = rows <= cols
            p1 = jnp.where(keep, p1, 0.0)
            p2 = jnp.where(keep, p2, 0.0)
        w = (p1 - p2).astype(BF16)
        d1 = (p1 * (dp - st[h, qs, 2:3])).astype(BF16)
        d2 = (p2 * (dp - st[h, qs, 3:4])).astype(BF16)
        kt = jnp.transpose(k)
        dqt[h, qs, 0:64] += dot(kt[0:64], d1)
        dqt[h, qs, 64:128] -= dot(kt[64:128], d2)
        dkv[h, ks, 0] += dot(d1, q1) + dot(d2, q2)
        dkv[h, ks, 1] += dot(w, do)

    def maybe_unit(h, i, j):
        qo = jnp.where(i < 2, i, 5 - i)
        ko = jnp.where(j < 2, j, 5 - j)
        qbase = jnp.where(h == 0, y, z)
        kbase = jnp.where(h == 0, z, y)
        qs = (qbase + qo) % 4
        ks = (kbase + ko) % 4
        q_block = jnp.where(h == 0, z * 4 + qs, qs * 4 + y)
        k_block = jnp.where(h == 0, ks * 4 + y, z * 4 + ks)

        @pl.when(k_block < q_block)
        def _():
            unit(h, qs, ks, False)

    unit(0, y, z, True)
    unit(1, z, y, True)

    second = []
    for some in (("q", "k"), ("v",), ("do", "st")):
        for axis in (0, 1):
            for name in some:
                for d in (0, 1):
                    first[axis, d, name].wait_recv()
                    if d == (0 if name in ("q", "k") else 1):
                        step = 1 if d == 0 else -1
                        ref = item(axis, name, ring(axis, -step))
                        n = 5 + names.index(name)
                        c = remote(ref, ref, gs.at[axis, d, n], gr.at[axis, d, n], peer(axis, step))
                        c.start()
                        second.append(c)

    def near_units(n, carry):
        h = n // 8
        m = n % 8 + 1
        maybe_unit(h, m // 3, m % 3)
        return carry

    lax.fori_loop(0, 16, near_units, 0)
    for c in second:
        c.wait_recv()

    def far_queries(n, carry):
        maybe_unit(n // 4, jnp.int32(3), n % 4)
        return carry

    def far_keys(n, carry):
        maybe_unit(n // 3, n % 3, jnp.int32(3))
        return carry

    class Reduction:
        def __init__(self, tx, rx, axis, base, get):
            self.tx, self.rx, self.axis, self.base, self.get = tx, rx, axis, base, get
            self.out = {}

        def go(self, j, value, step):
            axis = self.axis
            self.tx[axis, j] = value.astype(BF16)
            c = remote(
                self.tx.at[axis, j], self.rx.at[axis, j],
                rs.at[axis, self.base + j], rr.at[axis, self.base + j], peer(axis, step),
            )
            c.start()
            self.out[j] = c

        def far(self):
            slot = ring(self.axis, 2)
            self.go(0, self.get(slot, 0), 1)
            self.go(1, self.get(slot, 1), -1)

        def direct(self):
            self.go(2, self.get(ring(self.axis, 1), 1), 1)
            self.go(3, self.get(ring(self.axis, -1), 0), -1)

        def summed(self):
            for j, step in ((0, 1), (1, -1)):
                mine = self.get(ring(self.axis, step), j)
                self.out[j].wait_recv()
                self.go(4 + j, mine + self.rx[self.axis, j].astype(F32), step)

        def end(self):
            own0 = self.get(pos[self.axis], 0)
            own1 = self.get(pos[self.axis], 1)
            for j in (2, 3, 4, 5):
                self.out[j].wait_recv()
            rx = self.rx
            r0 = own0 + rx[self.axis, 3].astype(F32) + rx[self.axis, 4].astype(F32)
            r1 = own1 + rx[self.axis, 2].astype(F32) + rx[self.axis, 5].astype(F32)
            return r0, r1

        def drain(self):
            for c in self.out.values():
                c.wait_send()

    def get_dq(h):
        return lambda slot, p: dqt[h, slot, 64 * p : 64 * p + 64] * SCALE

    def get_dkv(h):
        return lambda slot, p: dkv[h, slot, p] * (SCALE if p == 0 else 1.0)

    def get_wg(h):
        def get(slot, p):
            parts = []
            for o in (2 * p, 2 * p + 1):
                blk = o * 4 + slot if h == 0 else slot * 4 + o
                cols = lat[:, pl.ds(pl.multiple_of(blk * T, T), T)]
                parts.append(dot(dqf[h], cols))
            return jnp.stack(parts)

        return get

    def get_last(h):
        def get(slot, p):
            start = pl.multiple_of(slot * 128 + 64 * p, 64)
            return jnp.concatenate(
                [wide[h, pl.ds(start, 64), :], wide[2 + h, pl.ds(start, 64), :]], axis=1
            )

        return get

    both = (0, 1)
    dq = [Reduction(qtx, qrx, h, 0, get_dq(h)) for h in both]
    dk = [Reduction(ktx, krx, 1 - h, 18, get_dkv(h)) for h in both]
    wa = [Reduction(atx, arx, h, 6, get_wg(h)) for h in both]
    wb = [Reduction(btx, brx, 1 - h, 12, get_last(h)) for h in both]

    lax.fori_loop(0, 8, far_queries, 0)
    for h in both:
        dq[h].far()
    lax.fori_loop(0, 6, far_keys, 0)
    for h in both:
        dq[h].direct()
    for h in both:
        dq[h].summed()
    for h in both:
        dk[h].far()
    for h in both:
        dk[h].direct()
    for h in both:
        dk[h].summed()
    loads[8].wait()
    for h in both:
        r0, r1 = dq[h].end()
        dqf[h, 0:64] = r0.astype(BF16)
        dqf[h, 64:128] = r1.astype(BF16)
        wa[h].far()
    for h in both:
        wa[h].direct()
    for h in both:
        wa[h].summed()
    for h in both:
        wide2[pl.ds(h, T, stride=2), :] = jnp.transpose(dqf[h].astype(F32))
    qg_ref[...] = wide2[0 : 2 * T, :].astype(BF16)
    stores = [
        pltpu.make_async_copy(a, b, out_sem.at[n])
        for n, (a, b) in enumerate(
            ((qg_ref, qg_hbm), (kg_ref, kg_hbm), (vg_ref, vg_hbm), (wg_ref, wg_hbm))
        )
    ]
    stores[0].start()
    for h in both:
        r0, r1 = wa[h].end()
        for o in range(4):
            part = r0[o] if o < 2 else r1[o - 2]
            wide[h, pl.ds(o * 128, 128), :] = part[:, 0:128]
            wide[2 + h, pl.ds(o * 128, 128), :] = part[:, 128:256]
        wb[h].far()
        wb[h].direct()
    for h in both:
        wb[h].summed()
    for p, ref in ((0, kg_ref), (1, vg_ref)):
        for h in both:
            if p == 0:
                ends = dk[h].end()
                dk[h].ends = ends
            wide2[pl.ds(2 * T * p + h, T, stride=2), :] = dk[h].ends[p]
        ref[...] = wide2[2 * T * p : 2 * T * p + 2 * T, :].astype(BF16)
        stores[1 + p].start()
    for h in both:
        r0, r1 = wb[h].end()
        wg_ref[:, h * W : h * W + W] = jnp.transpose(jnp.concatenate([r0, r1], axis=0))
    stores[3].start()

    for c in first.values():
        c.wait_send()
    for c in second:
        c.wait_send()
    for group in (dq, dk, wa, wb):
        for r in group:
            r.drain()
    for c in stores:
        c.wait()


def put_kernel(*refs):
    sources, targets, rooms, sems = refs[0:4], refs[4:8], refs[8:12], refs[12]
    reads = [pltpu.make_async_copy(sources[n], rooms[n], sems.at[n]) for n in range(4)]
    writes = [pltpu.make_async_copy(rooms[n], targets[n], sems.at[4 + n]) for n in range(4)]
    for c in reads:
        c.start()
    for n in range(4):
        reads[n].wait()
        writes[n].start()
    for c in writes:
        c.wait()


def body(latents, query_heads, key_heads, value_heads, map_outputs, log_sums, out_grad, mix_lambda, norm_gain):
    rows = 2 * T
    hbm = pl.BlockSpec(memory_space=pltpu.HBM)
    out_shape = (
        jax.ShapeDtypeStruct((rows, W), BF16),
        jax.ShapeDtypeStruct((rows, W), BF16),
        jax.ShapeDtypeStruct((rows, W), BF16),
        jax.ShapeDtypeStruct((T, 2 * W), F32),
    )
    outs = pl.pallas_call(
        kernel,
        out_shape=out_shape,
        in_specs=[hbm] * 9,
        out_specs=(hbm, hbm, hbm, hbm),
        scratch_shapes=[
            pltpu.VMEM((rows, W), BF16),
            pltpu.VMEM((rows, W), BF16),
            pltpu.VMEM((rows, W), BF16),
            pltpu.VMEM((2 * rows, W), BF16),
            pltpu.VMEM((2, 2, T), F32),
            pltpu.VMEM((rows, W), BF16),
            pltpu.SMEM((2,), F32),
            pltpu.VMEM((1, W), F32),
            pltpu.VMEM((T, 4096), BF16),
            pltpu.VMEM((2, 4, 2, T, W), BF16),
            pltpu.VMEM((2, 4, 2, T, W), BF16),
            pltpu.VMEM((2, 4, 8, T), F32),
            pltpu.VMEM((2, 4, W, T), F32),
            pltpu.VMEM((2, 4, 2, T, W), F32),
            pltpu.VMEM((4, rows, W), F32),
            pltpu.VMEM((4 * T, W), F32),
            pltpu.VMEM((2, W, T), BF16),
            pltpu.VMEM((2, 6, 64, T), BF16),
            pltpu.VMEM((2, 6, 64, T), BF16),
            pltpu.VMEM((2, 6, T, W), BF16),
            pltpu.VMEM((2, 6, T, W), BF16),
            pltpu.VMEM((2, 6, 2, W, T), BF16),
            pltpu.VMEM((2, 6, 2, W, T), BF16),
            pltpu.VMEM((2, 6, 64, T), BF16),
            pltpu.VMEM((2, 6, 64, T), BF16),
            pltpu.VMEM((rows, W), BF16),
            pltpu.VMEM((rows, W), BF16),
            pltpu.VMEM((rows, W), BF16),
            pltpu.VMEM((T, 2 * W), F32),
            pltpu.SemaphoreType.DMA((9,)),
            pltpu.SemaphoreType.DMA((4,)),
            pltpu.SemaphoreType.DMA((2, 2, 10)),
            pltpu.SemaphoreType.DMA((2, 2, 10)),
            pltpu.SemaphoreType.DMA((2, 24)),
            pltpu.SemaphoreType.DMA((2, 24)),
        ],
        compiler_params=pltpu.CompilerParams(
            collective_id=0, has_side_effects=True, vmem_limit_bytes=VMEM_ALL
        ),
    )(
        query_heads.reshape(rows, W),
        key_heads.reshape(rows, W),
        value_heads.reshape(rows, W),
        map_outputs.reshape(2 * rows, W),
        jnp.transpose(log_sums, (1, 2, 0)),
        out_grad.reshape(rows, W),
        mix_lambda,
        norm_gain.reshape(1, W),
        latents,
    )
    qg, kg, vg, wg = pl.pallas_call(
        put_kernel,
        out_shape=out_shape,
        in_specs=[hbm] * 4,
        out_specs=(hbm, hbm, hbm, hbm),
        scratch_shapes=[pltpu.VMEM(o.shape, o.dtype) for o in out_shape]
        + [pltpu.SemaphoreType.DMA((8,))],
        compiler_params=pltpu.CompilerParams(vmem_limit_bytes=VMEM_ALL),
    )(*outs)
    shape = query_heads.shape
    return (qg.reshape(shape), kg.reshape(shape), vg.reshape(shape), wg)


def solution(mesh):
    placed = (
        P("sp", None),
        P("sp", "tp", None),
        P("sp", "tp", None),
        P("sp", "tp", None),
        P("sp", None, "tp", None),
        P("sp", "tp", None),
        P("sp", "tp", None),
        P("tp"),
        P(),
    )
    return jax.shard_map(
        body,
        mesh=mesh,
        in_specs=placed,
        out_specs=(P("sp", "tp", None), P("sp", "tp", None), P("sp", "tp", None), P("sp", "tp")),
        check_vma=False,
    )
```

time: 67.1 us -> 55.5 us (0.83)
  local copies, waits for them, and re-layouts: 10.8 us -> 0 us
    unnamed x20 -> x0, local copies, waits for them, and re-layouts: 10.1 us -> none
    reshape x1 -> x0, local copies, waits for them, and re-layouts: 0.7 us -> none  [body(): jnp.transpose(log_sums, (1, 2, 0)).reshape(4, T)]
    pallas_call x1 -> x2, Pallas kernels: 55.3 us -> 54.7 us  [the longest x1 52.8 us: body(): pl.pallas_call(kernel, out_shape=out_shape, in_specs=[hbm] * 9, out_specs...]
where the time goes in v2:
time: 55.5 us; the launch traced here: 55.3 us
  Pallas kernels  54.7 us (99%)
  between operations  0.64 us (1%)
    pallas_call x1, Pallas kernels, body(): pl.pallas_call(kernel, out_shape=out_shape, in_specs=[hbm] * 9, out_specs...  52.8 us
    pallas_call x1, Pallas kernels, body(): pl.pallas_call(put_kernel, out_shape=out_shape, in_specs=[hbm] * 4, out_s...  1.92 us

profile of v2, /device:TPU:0, one launch (start us, length us, event | category | flops | bytes accessed | tf_op | source)
XLA Modules:
  0.0 55.3 jit_solution(4876281268813927237)
XLA Ops:
  0.6 52.8 %shard_map.120 = (bf16[512,128]{1,0:T(8,128)(2,1)}, bf16[512,128]{1,0:T(8,128)(2,1)}, bf16[512,128]{1,0:T(8,128)(2,1)}, f32[256,256]{1,0:T(8,128)}) custom-call(bf16[512,128]{1,0:T(8,128)(2,1)} %bitcast.11, bf16[512,128]{1,0:T(8,128)(2,1)} %bitcast.12, bf16[512,128]{1,0:T(8,128)(2,1)} %bitcast.13, bf16[1024,128]{1,0:T(8,128)(2,1)} %bitcast.10, ...), custom_call_target="tpu_custom_call" | custom-call | tf_op jit(solution)/shard_map/pallas_call | solution.py:383
  53.4 1.9 %shard_map.121 = (bf16[512,128]{1,0:T(8,128)(2,1)}, bf16[512,128]{1,0:T(8,128)(2,1)}, bf16[512,128]{1,0:T(8,128)(2,1)}, f32[256,256]{1,0:T(8,128)}) custom-call(bf16[512,128]{1,0:T(8,128)(2,1)} %get-tuple-element.12.refs_0_, bf16[512,128]{1,0:T(8,128)(2,1)} %get-tuple-element.13.refs_1_, bf16[512,128]{1,0:T(8,128)(2,1)} %get-tuple-element.14.refs_2_, ...), custom_call_target="tpu_custom_call" | custom-call | tf_op jit(solution)/shard_map/pallas_call | solution.py:439

commit v3 on v2

--- a/solution.py
+++ b/solution.py
@@ -14,7 +14,7 @@
 SCALE = 0.125
 T = 256
 W = 128
-VMEM_ALL = 67043328
+VMEM_ALL = 66200000
 NT = (((1,), (1,)), ((), ()))
 
 
@@ -28,12 +28,11 @@
 
 def kernel(
     q_hbm, k_hbm, v_hbm, mo_hbm, lse_hbm, og_hbm, lam_hbm, gain_hbm, lat_hbm,
-    qg_hbm, kg_hbm, vg_hbm, wg_hbm,
+    qg_ref, kg_ref, vg_ref, wg_ref,
     q_in, k_in, v_in, mo_in, lse_in, og_in, lam_in, gain_in,
-    lat, qdo, kv, st, dqt, dkv, wide, wide2, dqf,
+    lat, qdo, kv, st, dqt, dkv, wds, wide, wide2, dqf,
     qtx, qrx, ktx, krx, atx, arx, btx, brx,
-    qg_ref, kg_ref, vg_ref, wg_ref,
-    in_sem, out_sem, gs, gr, rs, rr,
+    in_sem, gs, gr, rs, rr,
 ):
     sp = lax.axis_index("sp")
     tp = lax.axis_index("tp")
@@ -137,35 +136,43 @@
 
     lane = lax.broadcasted_iota(jnp.int32, (T, W), 1)
 
-    def unit(h, qs, ks, masked):
+    def split_queries(h, qs):
         q = qdo[h, qs, 0]
+        zero = jnp.zeros_like(q)
+        return jnp.where(lane < 64, q, zero), jnp.where(lane < 64, zero, -q)
+
+    def scores(h, qs, ks, masked):
+        q1, q2 = split_queries(h, qs)
         do = qdo[h, qs, 1]
-        k = kv[h, ks, 0]
-        v = kv[h, ks, 1]
-        zero = jnp.zeros_like(q)
-        q1 = jnp.where(lane < 64, q, zero)
-        q2 = jnp.where(lane < 64, zero, -q)
-        s1 = dot_nt(k, q1)
-        s2 = dot_nt(k, q2)
-        dp = dot_nt(v, do)
-        p1 = jnp.exp2(s1 * (SCALE * LOG2E) - st[h, qs, 0:1])
-        p2 = jnp.exp2(s2 * (-SCALE * LOG2E) - st[h, qs, 1:2])
-        if masked:
-            rows = lax.broadcasted_iota(jnp.int32, (T, T), 0)
-            cols = lax.broadcasted_iota(jnp.int32, (T, T), 1)
-            keep = rows <= cols
-            p1 = jnp.where(keep, p1, 0.0)
-            p2 = jnp.where(keep, p2, 0.0)
-        w = (p1 - p2).astype(BF16)
-        d1 = (p1 * (dp - st[h, qs, 2:3])).astype(BF16)
-        d2 = (p2 * (dp - st[h, qs, 3:4])).astype(BF16)
-        kt = jnp.transpose(k)
+        half = T // 2
+        for c in (0, half):
+            k = kv[h, ks, 0, c : c + half]
+            v = kv[h, ks, 1, c : c + half]
+            s1 = dot_nt(k, q1)
+            s2 = dot_nt(k, q2)
+            dp = dot_nt(v, do)
+            p1 = jnp.exp2(s1 * (SCALE * LOG2E) - st[h, qs, 0:1])
+            p2 = jnp.exp2(s2 * (-SCALE * LOG2E) - st[h, qs, 1:2])
+            if masked:
+                rows = lax.broadcasted_iota(jnp.int32, (half, T), 0) + c
+                cols = lax.broadcasted_iota(jnp.int32, (half, T), 1)
+                keep = rows <= cols
+                p1 = jnp.where(keep, p1, 0.0)
+                p2 = jnp.where(keep, p2, 0.0)
+            wds[0, c : c + half] = (p1 - p2).astype(BF16)
+            wds[1, c : c + half] = (p1 * (dp - st[h, qs, 2:3])).astype(BF16)
+            wds[2, c : c + half] = (p2 * (dp - st[h, qs, 3:4])).astype(BF16)
+
+    def products(h, qs, ks):
+        q1, q2 = split_queries(h, qs)
+        w, d1, d2 = wds[0], wds[1], wds[2]
+        kt = jnp.transpose(kv[h, ks, 0])
         dqt[h, qs, 0:64] += dot(kt[0:64], d1)
         dqt[h, qs, 64:128] -= dot(kt[64:128], d2)
         dkv[h, ks, 0] += dot(d1, q1) + dot(d2, q2)
-        dkv[h, ks, 1] += dot(w, do)
-
-    def maybe_unit(h, i, j):
+        dkv[h, ks, 1] += dot(w, qdo[h, qs, 1])
+
+    def maybe_unit(h, i, j, before):
         qo = jnp.where(i < 2, i, 5 - i)
         ko = jnp.where(j < 2, j, 5 - j)
         qbase = jnp.where(h == 0, y, z)
@@ -174,13 +181,28 @@
         ks = (kbase + ko) % 4
         q_block = jnp.where(h == 0, z * 4 + qs, qs * 4 + y)
         k_block = jnp.where(h == 0, ks * 4 + y, z * 4 + ks)
-
-        @pl.when(k_block < q_block)
+        wanted = k_block < q_block
+
+        @pl.when(wanted)
         def _():
-            unit(h, qs, ks, False)
-
-    unit(0, y, z, True)
-    unit(1, z, y, True)
+            products(*before)
+            scores(h, qs, ks, False)
+
+        return tuple(jnp.where(wanted, a, b) for a, b in zip((h, qs, ks), before))
+
+    def some_units(count, which, before, fresh):
+        if fresh:
+            wds[...] = jnp.zeros_like(wds)
+
+        def step(n, carry):
+            return maybe_unit(*which(n), carry)
+
+        return lax.fori_loop(0, count, step, before)
+
+    scores(0, y, z, True)
+    products(0, y, z)
+    scores(1, z, y, True)
+    pending = (jnp.int32(1), z, y)
 
     second = []
     for some in (("q", "k"), ("v",), ("do", "st")):
@@ -196,23 +218,9 @@
                         c.start()
                         second.append(c)
 
-    def near_units(n, carry):
-        h = n // 8
-        m = n % 8 + 1
-        maybe_unit(h, m // 3, m % 3)
-        return carry
-
-    lax.fori_loop(0, 16, near_units, 0)
+    pending = some_units(16, lambda n: (n // 8, (n % 8 + 1) // 3, (n % 8 + 1) % 3), pending, False)
     for c in second:
         c.wait_recv()
-
-    def far_queries(n, carry):
-        maybe_unit(n // 4, jnp.int32(3), n % 4)
-        return carry
-
-    def far_keys(n, carry):
-        maybe_unit(n // 3, n % 3, jnp.int32(3))
-        return carry
 
     class Reduction:
         def __init__(self, tx, rx, axis, base, get):
@@ -290,18 +298,20 @@
     wa = [Reduction(atx, arx, h, 6, get_wg(h)) for h in both]
     wb = [Reduction(btx, brx, 1 - h, 12, get_last(h)) for h in both]
 
-    lax.fori_loop(0, 8, far_queries, 0)
+    pending = some_units(8, lambda n: (n // 4, jnp.int32(3), n % 4), pending, False)
+    products(*pending)
     for h in both:
         dq[h].far()
-    lax.fori_loop(0, 6, far_keys, 0)
+    for h in both:
+        dk[h].direct()
+    pending = some_units(6, lambda n: (n // 3, n % 3, jnp.int32(3)), pending, True)
+    products(*pending)
     for h in both:
         dq[h].direct()
     for h in both:
         dq[h].summed()
     for h in both:
         dk[h].far()
-    for h in both:
-        dk[h].direct()
     for h in both:
         dk[h].summed()
     loads[8].wait()
@@ -317,13 +327,6 @@
     for h in both:
         wide2[pl.ds(h, T, stride=2), :] = jnp.transpose(dqf[h].astype(F32))
     qg_ref[...] = wide2[0 : 2 * T, :].astype(BF16)
-    stores = [
-        pltpu.make_async_copy(a, b, out_sem.at[n])
-        for n, (a, b) in enumerate(
-            ((qg_ref, qg_hbm), (kg_ref, kg_hbm), (vg_ref, vg_hbm), (wg_ref, wg_hbm))
-        )
-    ]
-    stores[0].start()
     for h in both:
         r0, r1 = wa[h].end()
         for o in range(4):
@@ -341,11 +344,9 @@
                 dk[h].ends = ends
             wide2[pl.ds(2 * T * p + h, T, stride=2), :] = dk[h].ends[p]
         ref[...] = wide2[2 * T * p : 2 * T * p + 2 * T, :].astype(BF16)
-        stores[1 + p].start()
     for h in both:
         r0, r1 = wb[h].end()
         wg_ref[:, h * W : h * W + W] = jnp.transpose(jnp.concatenate([r0, r1], axis=0))
-    stores[3].start()
 
     for c in first.values():
         c.wait_send()
@@ -354,26 +355,21 @@
     for group in (dq, dk, wa, wb):
         for r in group:
             r.drain()
-    for c in stores:
-        c.wait()
 
 
 def put_kernel(*refs):
-    sources, targets, rooms, sems = refs[0:4], refs[4:8], refs[8:12], refs[12]
-    reads = [pltpu.make_async_copy(sources[n], rooms[n], sems.at[n]) for n in range(4)]
-    writes = [pltpu.make_async_copy(rooms[n], targets[n], sems.at[4 + n]) for n in range(4)]
-    for c in reads:
+    sems = refs[8]
+    copies = [pltpu.make_async_copy(refs[n], refs[4 + n], sems.at[n]) for n in range(4)]
+    for c in copies:
         c.start()
-    for n in range(4):
-        reads[n].wait()
-        writes[n].start()
-    for c in writes:
+    for c in copies:
         c.wait()
 
 
 def body(latents, query_heads, key_heads, value_heads, map_outputs, log_sums, out_grad, mix_lambda, norm_gain):
     rows = 2 * T
     hbm = pl.BlockSpec(memory_space=pltpu.HBM)
+    vmem = pl.BlockSpec(memory_space=pltpu.VMEM)
     out_shape = (
         jax.ShapeDtypeStruct((rows, W), BF16),
         jax.ShapeDtypeStruct((rows, W), BF16),
@@ -382,9 +378,9 @@
     )
     outs = pl.pallas_call(
         kernel,
-        out_shape=out_shape,
+        out_shape=tuple(pltpu.VMEM(o.shape, o.dtype) for o in out_shape),
         in_specs=[hbm] * 9,
-        out_specs=(hbm, hbm, hbm, hbm),
+        out_specs=(vmem, vmem, vmem, vmem),
         scratch_shapes=[
             pltpu.VMEM((rows, W), BF16),
             pltpu.VMEM((rows, W), BF16),
@@ -400,6 +396,7 @@
             pltpu.VMEM((2, 4, 8, T), F32),
             pltpu.VMEM((2, 4, W, T), F32),
             pltpu.VMEM((2, 4, 2, T, W), F32),
+            pltpu.VMEM((3, T, T), BF16),
             pltpu.VMEM((4, rows, W), F32),
             pltpu.VMEM((4 * T, W), F32),
             pltpu.VMEM((2, W, T), BF16),
@@ -411,12 +408,7 @@
             pltpu.VMEM((2, 6, 2, W, T), BF16),
             pltpu.VMEM((2, 6, 64, T), BF16),
             pltpu.VMEM((2, 6, 64, T), BF16),
-            pltpu.VMEM((rows, W), BF16),
-            pltpu.VMEM((rows, W), BF16),
-            pltpu.VMEM((rows, W), BF16),
-            pltpu.VMEM((T, 2 * W), F32),
             pltpu.SemaphoreType.DMA((9,)),
-            pltpu.SemaphoreType.DMA((4,)),
             pltpu.SemaphoreType.DMA((2, 2, 10)),
             pltpu.SemaphoreType.DMA((2, 2, 10)),
             pltpu.SemaphoreType.DMA((2, 24)),
@@ -439,11 +431,10 @@
     qg, kg, vg, wg = pl.pallas_call(
         put_kernel,
         out_shape=out_shape,
-        in_specs=[hbm] * 4,
+        in_specs=[vmem] * 4,
         out_specs=(hbm, hbm, hbm, hbm),
-        scratch_shapes=[pltpu.VMEM(o.shape, o.dtype) for o in out_shape]
-        + [pltpu.SemaphoreType.DMA((8,))],
-        compiler_params=pltpu.CompilerParams(vmem_limit_bytes=VMEM_ALL),
+        scratch_shapes=[pltpu.SemaphoreType.DMA((4,))],
+        compiler_params=pltpu.CompilerParams(vmem_limit_bytes=1024 * 1024),
     )(*outs)
     shape = query_heads.shape
     return (qg.reshape(shape), kg.reshape(shape), vg.reshape(shape), wg)

time: 55.5 us -> 51.7 us (0.932)
  Pallas kernels: 54.7 us -> 51 us
    pallas_call x2, Pallas kernels: 54.7 us -> 51 us  [the longest x1 50.1 us: body(): pl.pallas_call(kernel, out_shape=tuple((pltpu.VMEM(o.shape, o.dtype) for...]
where the time goes in v3:
time: 51.7 us; the launch traced here: 51.6 us
  Pallas kernels  51 us (99%)
  between operations  0.64 us (1%)
    pallas_call x1, Pallas kernels, body(): pl.pallas_call(kernel, out_shape=tuple((pltpu.VMEM(o.shape, o.dtype) for...  50.1 us

profile of v3, /device:TPU:0, one launch (start us, length us, event | category | flops | bytes accessed | tf_op | source)
XLA Modules:
  0.0 51.6 jit_solution(1907018043222131784)
XLA Ops:
  0.6 50.1 %shard_map.120 = (bf16[512,128]{1,0:T(8,128)(2,1)S(1)}, bf16[512,128]{1,0:T(8,128)(2,1)S(1)}, bf16[512,128]{1,0:T(8,128)(2,1)S(1)}, f32[256,256]{1,0:T(8,128)S(1)}) custom-call(bf16[512,128]{1,0:T(8,128)(2,1)} %bitcast.11, bf16[512,128]{1,0:T(8,128)(2,1)} %bitcast.12, bf16[512,128]{1,0:T(8,128)(2,1)} %bitcast.13, bf16[1024,128]{1,0:T(8,128)(2,1)} %bitcast.10, ...), custom_call_target="tpu_custom_call" | custom-call | tf_op jit(solution)/shard_map/pallas_call | solution.py:379
  50.7 0.9 %shard_map.121 = (bf16[512,128]{1,0:T(8,128)(2,1)}, bf16[512,128]{1,0:T(8,128)(2,1)}, bf16[512,128]{1,0:T(8,128)(2,1)}, f32[256,256]{1,0:T(8,128)}) custom-call(bf16[512,128]{1,0:T(8,128)(2,1)S(1)} %get-tuple-element.12.refs_0_, bf16[512,128]{1,0:T(8,128)(2,1)S(1)} %get-tuple-element.13.refs_1_, bf16[512,128]{1,0:T(8,128)(2,1)S(1)} %get-tuple-element.14.refs_2_, ...), custom_call_target="tpu_custom_call" | custom-call | tf_op jit(solution)/shard_map/pallas_call | solution.py:431

commit v4 on v3

--- a/solution.py
+++ b/solution.py
@@ -30,9 +30,9 @@
     q_hbm, k_hbm, v_hbm, mo_hbm, lse_hbm, og_hbm, lam_hbm, gain_hbm, lat_hbm,
     qg_ref, kg_ref, vg_ref, wg_ref,
     q_in, k_in, v_in, mo_in, lse_in, og_in, lam_in, gain_in,
-    lat, qdo, kv, st, dqt, dkv, wds, wide, wide2, dqf,
-    qtx, qrx, ktx, krx, atx, arx, btx, brx,
-    in_sem, gs, gr, rs, rr,
+    lat, lx, qdo, kv, st, dqt, dkv, wds, wide, wide2, dqf, dqg,
+    qtx, qrx, ktx, krx, etx, erx, btx, brx,
+    in_sem, gs, gr, rs, rr, ls, lr, ds, dr, hs, hr, es, er,
 ):
     sp = lax.axis_index("sp")
     tp = lax.axis_index("tp")
@@ -53,15 +53,26 @@
             device_id=device, device_id_type=pl.DeviceIdType.MESH,
         )
 
+    def role_step(axis, role):
+        sign = 1 - 2 * (pos[axis] % 2)
+        return sign if role == 0 else -sign
+
+    core = tp % 2
+    sibling = (sp, tp + 1 - 2 * core)
     barrier = pltpu.get_barrier_semaphore()
+    pl.semaphore_signal(barrier, inc=1, device_id=sibling, device_id_type=pl.DeviceIdType.MESH)
     for axis in (0, 1):
         for step in (1, -1):
             pl.semaphore_signal(
                 barrier, inc=1, device_id=peer(axis, step), device_id_type=pl.DeviceIdType.MESH
             )
-    sources = (q_hbm, k_hbm, v_hbm, og_hbm, mo_hbm, lse_hbm, lam_hbm, gain_hbm, lat_hbm)
-    targets = (q_in, k_in, v_in, og_in, mo_in, lse_in, lam_in, gain_in, lat)
+    sources = (q_hbm, k_hbm, v_hbm, og_hbm, mo_hbm, lse_hbm, lam_hbm, gain_hbm)
+    targets = (q_in, k_in, v_in, og_in, mo_in, lse_in, lam_in, gain_in)
     loads = [pltpu.make_async_copy(a, b, in_sem.at[n]) for n, (a, b) in enumerate(zip(sources, targets))]
+    loads += [
+        pltpu.make_async_copy(lat_hbm.at[:, n * T : n * T + T], lat.at[n // 4, n % 4], in_sem.at[8 + n])
+        for n in range(16)
+    ]
     for c in loads:
         c.start()
 
@@ -74,7 +85,7 @@
         qdo[h, qpos[h], 0] = wide[0, pl.ds(h, T, stride=2), :].astype(BF16)
         kv[h, kpos[h], 0] = wide[1, pl.ds(h, T, stride=2), :].astype(BF16)
         kv[h, kpos[h], 1] = wide[2, pl.ds(h, T, stride=2), :].astype(BF16)
-    pl.semaphore_wait(barrier, 4)
+    pl.semaphore_wait(barrier, 5)
 
     qh = (0, 1)
     kh = (1, 0)
@@ -218,6 +229,23 @@
                         c.start()
                         second.append(c)
 
+    for c in loads[8:]:
+        c.wait()
+    rows = pl.ds(pl.multiple_of(core * 128, 128), 128)
+    shares = []
+    for axis in (0, 1):
+        for role in (0, 1):
+            step = role_step(axis, role)
+            for w, owner in enumerate((ring(axis, step), ring(axis, 2))):
+                some = slice(2 * role, 2 * role + 2)
+                src = lat.at[some, owner, rows, :] if axis == 0 else lat.at[owner, some, rows, :]
+                c = remote(
+                    src, lx.at[axis, role, w, :, rows, :], ls.at[axis, role, w], lr.at[axis, role, w],
+                    peer(axis, step),
+                )
+                c.start()
+                shares.append(c)
+
     pending = some_units(16, lambda n: (n // 8, (n % 8 + 1) // 3, (n % 8 + 1) % 3), pending, False)
     for c in second:
         c.wait_recv()
@@ -272,17 +300,6 @@
     def get_dkv(h):
         return lambda slot, p: dkv[h, slot, p] * (SCALE if p == 0 else 1.0)
 
-    def get_wg(h):
-        def get(slot, p):
-            parts = []
-            for o in (2 * p, 2 * p + 1):
-                blk = o * 4 + slot if h == 0 else slot * 4 + o
-                cols = lat[:, pl.ds(pl.multiple_of(blk * T, T), T)]
-                parts.append(dot(dqf[h], cols))
-            return jnp.stack(parts)
-
-        return get
-
     def get_last(h):
         def get(slot, p):
             start = pl.multiple_of(slot * 128 + 64 * p, 64)
@@ -295,7 +312,6 @@
     both = (0, 1)
     dq = [Reduction(qtx, qrx, h, 0, get_dq(h)) for h in both]
     dk = [Reduction(ktx, krx, 1 - h, 18, get_dkv(h)) for h in both]
-    wa = [Reduction(atx, arx, h, 6, get_wg(h)) for h in both]
     wb = [Reduction(btx, brx, 1 - h, 12, get_last(h)) for h in both]
 
     pending = some_units(8, lambda n: (n // 4, jnp.int32(3), n % 4), pending, False)
@@ -312,38 +328,83 @@
         dq[h].summed()
     for h in both:
         dk[h].far()
-    for h in both:
-        dk[h].summed()
-    loads[8].wait()
+    def block(h, owner, o):
+        return lat[o, owner] if h == 0 else lat[owner, o]
+
+    def term(h, role, w, owner, o):
+        near = dot(dqf[h], block(h, owner, 2 * role + o))
+        return near + dot(dqg[h, role], lx[h, role, w, o])
+
+    hands = {}
     for h in both:
         r0, r1 = dq[h].end()
         dqf[h, 0:64] = r0.astype(BF16)
         dqf[h, 64:128] = r1.astype(BF16)
-        wa[h].far()
-    for h in both:
-        wa[h].direct()
-    for h in both:
-        wa[h].summed()
+        for role in both:
+            c = remote(
+                dqf.at[h], dqg.at[h, role], hs.at[h, role], hr.at[h, role], peer(h, role_step(h, role))
+            )
+            c.start()
+            hands[h, role] = c
+    swaps = []
+    for c in shares:
+        c.wait_recv()
+    for axis in (0, 1):
+        for role in (0, 1):
+            ref = lx.at[axis, role, :, :, rows, :]
+            c = remote(ref, ref, ds.at[axis, role], dr.at[axis, role], sibling)
+            c.start()
+            swaps.append(c)
+    for h in both:
+        dk[h].summed()
+    for c in swaps:
+        c.wait_recv()
+    odd = [pos[1 - h] % 2 for h in both]
+    trades = {}
+    for h in both:
+        for role in both:
+            step = role_step(h, 1 - role)
+            hands[h, role].wait_recv()
+            for n, o in enumerate((odd[h], 1 - odd[h])):
+                etx[h, role, n] = term(h, role, 1, ring(h, step), o).astype(BF16)
+                c = remote(
+                    etx.at[h, role, n], erx.at[h, role, n], es.at[h, role, n], er.at[h, role, n],
+                    peer(h, step),
+                )
+                c.start()
+                trades[h, role, n] = c
+
+    def place(h, slot):
+        return pl.ds(pl.multiple_of(slot * 128, 128), 128)
+
+    for h in both:
+        for role in both:
+            for o in both:
+                part = term(h, role, 0, pos[h], o)
+                wide[h, place(h, 2 * role + o), :] = part[:, 0:128]
+                wide[2 + h, place(h, 2 * role + o), :] = part[:, 128:256]
     for h in both:
         wide2[pl.ds(h, T, stride=2), :] = jnp.transpose(dqf[h].astype(F32))
     qg_ref[...] = wide2[0 : 2 * T, :].astype(BF16)
-    for h in both:
-        r0, r1 = wa[h].end()
-        for o in range(4):
-            part = r0[o] if o < 2 else r1[o - 2]
-            wide[h, pl.ds(o * 128, 128), :] = part[:, 0:128]
-            wide[2 + h, pl.ds(o * 128, 128), :] = part[:, 128:256]
-        wb[h].far()
-        wb[h].direct()
-    for h in both:
-        wb[h].summed()
+    ends = [dk[h].end() for h in both]
     for p, ref in ((0, kg_ref), (1, vg_ref)):
         for h in both:
-            if p == 0:
-                ends = dk[h].end()
-                dk[h].ends = ends
-            wide2[pl.ds(2 * T * p + h, T, stride=2), :] = dk[h].ends[p]
+            wide2[pl.ds(2 * T * p + h, T, stride=2), :] = ends[h][p]
         ref[...] = wide2[2 * T * p : 2 * T * p + 2 * T, :].astype(BF16)
+    for n in both:
+        for h in both:
+            o = odd[h] if n == 0 else 1 - odd[h]
+            for role in both:
+                trades[h, role, n].wait_recv()
+                got = erx[h, role, n].astype(F32)
+                wide[h, place(h, 2 * role + o), :] += got[:, 0:128]
+                wide[2 + h, place(h, 2 * role + o), :] += got[:, 128:256]
+            if n == 0:
+                wb[h].far()
+            else:
+                wb[h].direct()
+    for h in both:
+        wb[h].summed()
     for h in both:
         r0, r1 = wb[h].end()
         wg_ref[:, h * W : h * W + W] = jnp.transpose(jnp.concatenate([r0, r1], axis=0))
@@ -352,7 +413,9 @@
         c.wait_send()
     for c in second:
         c.wait_send()
-    for group in (dq, dk, wa, wb):
+    for c in shares + swaps + list(hands.values()) + list(trades.values()):
+        c.wait_send()
+    for group in (dq, dk, wb):
         for r in group:
             r.drain()
 
@@ -390,7 +453,8 @@
             pltpu.VMEM((rows, W), BF16),
             pltpu.SMEM((2,), F32),
             pltpu.VMEM((1, W), F32),
-            pltpu.VMEM((T, 4096), BF16),
+            pltpu.VMEM((4, 4, T, T), BF16),
+            pltpu.VMEM((2, 2, 2, 2, T, T), BF16),
             pltpu.VMEM((2, 4, 2, T, W), BF16),
             pltpu.VMEM((2, 4, 2, T, W), BF16),
             pltpu.VMEM((2, 4, 8, T), F32),
@@ -400,19 +464,28 @@
             pltpu.VMEM((4, rows, W), F32),
             pltpu.VMEM((4 * T, W), F32),
             pltpu.VMEM((2, W, T), BF16),
+            pltpu.VMEM((2, 2, W, T), BF16),
             pltpu.VMEM((2, 6, 64, T), BF16),
             pltpu.VMEM((2, 6, 64, T), BF16),
             pltpu.VMEM((2, 6, T, W), BF16),
             pltpu.VMEM((2, 6, T, W), BF16),
-            pltpu.VMEM((2, 6, 2, W, T), BF16),
-            pltpu.VMEM((2, 6, 2, W, T), BF16),
+            pltpu.VMEM((2, 2, 2, W, T), BF16),
+            pltpu.VMEM((2, 2, 2, W, T), BF16),
             pltpu.VMEM((2, 6, 64, T), BF16),
             pltpu.VMEM((2, 6, 64, T), BF16),
-            pltpu.SemaphoreType.DMA((9,)),
+            pltpu.SemaphoreType.DMA((24,)),
             pltpu.SemaphoreType.DMA((2, 2, 10)),
             pltpu.SemaphoreType.DMA((2, 2, 10)),
             pltpu.SemaphoreType.DMA((2, 24)),
             pltpu.SemaphoreType.DMA((2, 24)),
+            pltpu.SemaphoreType.DMA((2, 2, 2)),
+            pltpu.SemaphoreType.DMA((2, 2, 2)),
+            pltpu.SemaphoreType.DMA((2, 2)),
+            pltpu.SemaphoreType.DMA((2, 2)),
+            pltpu.SemaphoreType.DMA((2, 2)),
+            pltpu.SemaphoreType.DMA((2, 2)),
+            pltpu.SemaphoreType.DMA((2, 2, 2)),
+            pltpu.SemaphoreType.DMA((2, 2, 2)),
         ],
         compiler_params=pltpu.CompilerParams(
             collective_id=0, has_side_effects=True, vmem_limit_bytes=VMEM_ALL

time: 51.7 us -> 46.9 us (0.907)
  Pallas kernels: 51 us -> 46.2 us
    pallas_call x1, Pallas kernels: 50.1 us -> 45.3 us  [body(): pl.pallas_call(kernel, out_shape=tuple((pltpu.VMEM(o.shape, o.dtype) for...]
where the time goes in v4:
time: 46.9 us; the launch traced here: 46.8 us
  Pallas kernels  46.2 us (99%)
  between operations  0.64 us (1%)
    pallas_call x1, Pallas kernels, body(): pl.pallas_call(kernel, out_shape=tuple((pltpu.VMEM(o.shape, o.dtype) for...  45.3 us

profile of v4, /device:TPU:0, one launch (start us, length us, event | category | flops | bytes accessed | tf_op | source)
XLA Modules:
  0.0 46.8 jit_solution(11686806154307620048)
XLA Ops:
  0.6 45.3 %shard_map.120 = (bf16[512,128]{1,0:T(8,128)(2,1)S(1)}, bf16[512,128]{1,0:T(8,128)(2,1)S(1)}, bf16[512,128]{1,0:T(8,128)(2,1)S(1)}, f32[256,256]{1,0:T(8,128)S(1)}) custom-call(bf16[512,128]{1,0:T(8,128)(2,1)} %bitcast.11, bf16[512,128]{1,0:T(8,128)(2,1)} %bitcast.12, bf16[512,128]{1,0:T(8,128)(2,1)} %bitcast.13, bf16[1024,128]{1,0:T(8,128)(2,1)} %bitcast.10, ...), custom_call_target="tpu_custom_call" | custom-call | tf_op jit(solution)/shard_map/pallas_call | solution.py:442
  45.9 0.9 %shard_map.121 = (bf16[512,128]{1,0:T(8,128)(2,1)}, bf16[512,128]{1,0:T(8,128)(2,1)}, bf16[512,128]{1,0:T(8,128)(2,1)}, f32[256,256]{1,0:T(8,128)}) custom-call(bf16[512,128]{1,0:T(8,128)(2,1)S(1)} %get-tuple-element.12.refs_0_, bf16[512,128]{1,0:T(8,128)(2,1)S(1)} %get-tuple-element.13.refs_1_, bf16[512,128]{1,0:T(8,128)(2,1)S(1)} %get-tuple-element.14.refs_2_, ...), custom_call_target="tpu_custom_call" | custom-call | tf_op jit(solution)/shard_map/pallas_call | solution.py:504

commit v5 on v4

--- a/solution.py
+++ b/solution.py
@@ -31,7 +31,7 @@
     qg_ref, kg_ref, vg_ref, wg_ref,
     q_in, k_in, v_in, mo_in, lse_in, og_in, lam_in, gain_in,
     lat, lx, qdo, kv, st, dqt, dkv, wds, wide, wide2, dqf, dqg,
-    qtx, qrx, ktx, krx, etx, erx, btx, brx,
+    qtx, qrx, ktx, krx, etx, erx, btx, brx, pre,
     in_sem, gs, gr, rs, rr, ls, lr, ds, dr, hs, hr, es, er,
 ):
     sp = lax.axis_index("sp")
@@ -62,7 +62,7 @@
     barrier = pltpu.get_barrier_semaphore()
     pl.semaphore_signal(barrier, inc=1, device_id=sibling, device_id_type=pl.DeviceIdType.MESH)
     for axis in (0, 1):
-        for step in (1, -1):
+        for step in (1, -1, 2):
             pl.semaphore_signal(
                 barrier, inc=1, device_id=peer(axis, step), device_id_type=pl.DeviceIdType.MESH
             )
@@ -78,15 +78,6 @@
 
     qpos = (y, z)
     kpos = (z, y)
-    for n, ref in enumerate((q_in, k_in, v_in)):
-        loads[n].wait()
-        wide[n] = ref[...].astype(F32)
-    for h in (0, 1):
-        qdo[h, qpos[h], 0] = wide[0, pl.ds(h, T, stride=2), :].astype(BF16)
-        kv[h, kpos[h], 0] = wide[1, pl.ds(h, T, stride=2), :].astype(BF16)
-        kv[h, kpos[h], 1] = wide[2, pl.ds(h, T, stride=2), :].astype(BF16)
-    pl.semaphore_wait(barrier, 5)
-
     qh = (0, 1)
     kh = (1, 0)
     first = {}
@@ -104,17 +95,68 @@
 
     names = ("q", "k", "v", "do", "st")
 
+    def gather_copy(axis, d, name, slot, forward):
+        n = names.index(name) + (5 if forward else 0)
+        ref = item(axis, name, slot)
+        step = 1 if d == 0 else -1
+        return remote(ref, ref, gs.at[axis, d, n], gr.at[axis, d, n], peer(axis, step))
+
+    ups = ("k", "v")
+    downs = ("q", "do", "st")
+
+    def z_each(some, forward, do_it):
+        if forward:
+            middle = (z == 1) | (z == 2)
+            cases = ((0, middle, ups, -1), (1, middle, downs, 1))
+        else:
+            cases = ((0, z < 3, ups, 0), (0, z == 3, downs, 0), (1, z > 0, downs, 0), (1, z == 0, ups, 0))
+        for d, wanted, group, shift in cases:
+            mine = [name for name in some if name in group]
+            if mine:
+                @pl.when(wanted)
+                def _():
+                    for name in mine:
+                        do_it(gather_copy(1, d, name, ring(1, shift), forward))
+
+    def z_arrived(some, forward):
+        if forward:
+            cases = ((0, z >= 2, ups, 2), (1, z < 2, downs, 2))
+        else:
+            cases = ((0, z > 0, ups, -1), (0, z == 0, downs, -1), (1, z < 3, downs, 1), (1, z == 3, ups, 1))
+        for d, wanted, group, shift in cases:
+            mine = [name for name in some if name in group]
+            if mine:
+                @pl.when(wanted)
+                def _():
+                    for name in mine:
+                        gather_copy(1, d, name, ring(1, shift), forward).wait_recv()
+
+    def start(c):
+        c.start()
+
+    def wait_send(c):
+        c.wait_send()
+
     def send_own(some):
         for name in some:
-            for axis in (0, 1):
-                for d, step in enumerate((1, -1)):
-                    n = names.index(name)
-                    ref = item(axis, name, pos[axis])
-                    c = remote(ref, ref, gs.at[axis, d, n], gr.at[axis, d, n], peer(axis, step))
-                    c.start()
-                    first[axis, d, name] = c
-
-    send_own(("q", "k", "v"))
+            for d in (0, 1):
+                c = gather_copy(0, d, name, y, False)
+                c.start()
+                first[d, name] = c
+            z_each((name,), False, start)
+
+    for n, (name, ref) in enumerate((("q", q_in), ("k", k_in), ("v", v_in))):
+        loads[n].wait()
+        wide[n] = ref[...].astype(F32)
+        for h in (0, 1):
+            part = wide[n, pl.ds(h, T, stride=2), :].astype(BF16)
+            if n == 0:
+                qdo[h, qpos[h], 0] = part
+            else:
+                kv[h, kpos[h], n - 1] = part
+        if n == 0:
+            pl.semaphore_wait(barrier, 7)
+        send_own((name,))
 
     for c in loads[3:8]:
         c.wait()
@@ -217,17 +259,15 @@
 
     second = []
     for some in (("q", "k"), ("v",), ("do", "st")):
-        for axis in (0, 1):
-            for name in some:
-                for d in (0, 1):
-                    first[axis, d, name].wait_recv()
-                    if d == (0 if name in ("q", "k") else 1):
-                        step = 1 if d == 0 else -1
-                        ref = item(axis, name, ring(axis, -step))
-                        n = 5 + names.index(name)
-                        c = remote(ref, ref, gs.at[axis, d, n], gr.at[axis, d, n], peer(axis, step))
-                        c.start()
-                        second.append(c)
+        for name in some:
+            for d in (0, 1):
+                first[d, name].wait_recv()
+                if d == (0 if name in ("q", "k") else 1):
+                    c = gather_copy(0, d, name, ring(0, -1 if d == 0 else 1), True)
+                    c.start()
+                    second.append(c)
+        z_arrived(some, False)
+        z_each(some, True, start)
 
     for c in loads[8:]:
         c.wait()
@@ -247,6 +287,10 @@
                 shares.append(c)
 
     pending = some_units(16, lambda n: (n // 8, (n % 8 + 1) // 3, (n % 8 + 1) % 3), pending, False)
+    z_arrived(names, True)
+    pending = some_units(
+        6, lambda n: (n // 3, jnp.where(n < 3, n, 3), jnp.where(n < 3, 3, n - 3)), pending, False
+    )
     for c in second:
         c.wait_recv()
 
@@ -294,38 +338,69 @@
             for c in self.out.values():
                 c.wait_send()
 
+    class Direct:
+        def __init__(self, tx, rx, axis, base, get):
+            self.tx, self.rx, self.axis, self.base, self.get = tx, rx, axis, base, get
+            self.out = {}
+
+        def go(self, j, step):
+            axis = self.axis
+            self.tx[axis, j] = self.get(ring(axis, step)).astype(BF16)
+            c = remote(
+                self.tx.at[axis, j], self.rx.at[axis, j],
+                rs.at[axis, self.base + j], rr.at[axis, self.base + j], peer(axis, step),
+            )
+            c.start()
+            self.out[j] = c
+
+        def far(self):
+            self.go(0, 2)
+
+        def direct(self):
+            self.go(1, 1)
+            self.go(2, -1)
+
+        def end(self):
+            total = self.get(pos[self.axis])
+            for j in (1, 2, 0):
+                self.out[j].wait_recv()
+                total = total + self.rx[self.axis, j].astype(F32)
+            return total
+
+        def drain(self):
+            for c in self.out.values():
+                c.wait_send()
+
     def get_dq(h):
-        return lambda slot, p: dqt[h, slot, 64 * p : 64 * p + 64] * SCALE
+        return lambda slot: dqt[h, slot] * SCALE
 
     def get_dkv(h):
         return lambda slot, p: dkv[h, slot, p] * (SCALE if p == 0 else 1.0)
 
     def get_last(h):
-        def get(slot, p):
-            start = pl.multiple_of(slot * 128 + 64 * p, 64)
-            return jnp.concatenate(
-                [wide[h, pl.ds(start, 64), :], wide[2 + h, pl.ds(start, 64), :]], axis=1
-            )
+        def get(slot):
+            rows = pl.ds(pl.multiple_of(slot * 128, 128), 128)
+            return jnp.concatenate([wide[h, rows, :], wide[2 + h, rows, :]], axis=1)
 
         return get
 
     both = (0, 1)
-    dq = [Reduction(qtx, qrx, h, 0, get_dq(h)) for h in both]
+    dq = [Direct(qtx, qrx, h, 0, get_dq(h)) for h in both]
     dk = [Reduction(ktx, krx, 1 - h, 18, get_dkv(h)) for h in both]
-    wb = [Reduction(btx, brx, 1 - h, 12, get_last(h)) for h in both]
-
-    pending = some_units(8, lambda n: (n // 4, jnp.int32(3), n % 4), pending, False)
+    wb = [Direct(btx, brx, 1 - h, 12, get_last(h)) for h in both]
+
+    pending = some_units(
+        5, lambda n: (jnp.where(n == 0, 1, 0), jnp.int32(3), jnp.where(n == 0, 3, n - 1)), pending, False
+    )
     products(*pending)
     for h in both:
         dq[h].far()
+    dq[0].direct()
     for h in both:
         dk[h].direct()
-    pending = some_units(6, lambda n: (n // 3, n % 3, jnp.int32(3)), pending, True)
+    pending = some_units(3, lambda n: (jnp.int32(1), n, jnp.int32(3)), pending, True)
     products(*pending)
-    for h in both:
-        dq[h].direct()
-    for h in both:
-        dq[h].summed()
+    dq[1].direct()
     for h in both:
         dk[h].far()
     def block(h, owner, o):
@@ -337,9 +412,7 @@
 
     hands = {}
     for h in both:
-        r0, r1 = dq[h].end()
-        dqf[h, 0:64] = r0.astype(BF16)
-        dqf[h, 64:128] = r1.astype(BF16)
+        dqf[h] = dq[h].end().astype(BF16)
         for role in both:
             c = remote(
                 dqf.at[h], dqg.at[h, role], hs.at[h, role], hr.at[h, role], peer(h, role_step(h, role))
@@ -363,13 +436,18 @@
     trades = {}
     for h in both:
         for role in both:
-            step = role_step(h, 1 - role)
-            hands[h, role].wait_recv()
             for n, o in enumerate((odd[h], 1 - odd[h])):
-                etx[h, role, n] = term(h, role, 1, ring(h, step), o).astype(BF16)
+                pre[h, role, n] = dot(dqf[h], block(h, ring(h, role_step(h, 1 - role)), 2 * role + o))
+    for n in both:
+        for h in both:
+            o = odd[h] if n == 0 else 1 - odd[h]
+            for role in both:
+                if n == 0:
+                    hands[h, role].wait_recv()
+                etx[h, role, n] = (pre[h, role, n] + dot(dqg[h, role], lx[h, role, 1, o])).astype(BF16)
                 c = remote(
                     etx.at[h, role, n], erx.at[h, role, n], es.at[h, role, n], er.at[h, role, n],
-                    peer(h, step),
+                    peer(h, role_step(h, 1 - role)),
                 )
                 c.start()
                 trades[h, role, n] = c
@@ -404,15 +482,14 @@
             else:
                 wb[h].direct()
     for h in both:
-        wb[h].summed()
-    for h in both:
-        r0, r1 = wb[h].end()
-        wg_ref[:, h * W : h * W + W] = jnp.transpose(jnp.concatenate([r0, r1], axis=0))
+        wg_ref[:, h * W : h * W + W] = jnp.transpose(wb[h].end())
 
     for c in first.values():
         c.wait_send()
     for c in second:
         c.wait_send()
+    for forward in (False, True):
+        z_each(names, forward, wait_send)
     for c in shares + swaps + list(hands.values()) + list(trades.values()):
         c.wait_send()
     for group in (dq, dk, wb):
@@ -465,14 +542,15 @@
             pltpu.VMEM((4 * T, W), F32),
             pltpu.VMEM((2, W, T), BF16),
             pltpu.VMEM((2, 2, W, T), BF16),
-            pltpu.VMEM((2, 6, 64, T), BF16),
-            pltpu.VMEM((2, 6, 64, T), BF16),
+            pltpu.VMEM((2, 3, W, T), BF16),
+            pltpu.VMEM((2, 3, W, T), BF16),
             pltpu.VMEM((2, 6, T, W), BF16),
             pltpu.VMEM((2, 6, T, W), BF16),
             pltpu.VMEM((2, 2, 2, W, T), BF16),
             pltpu.VMEM((2, 2, 2, W, T), BF16),
-            pltpu.VMEM((2, 6, 64, T), BF16),
-            pltpu.VMEM((2, 6, 64, T), BF16),
+            pltpu.VMEM((2, 3, W, T), BF16),
+            pltpu.VMEM((2, 3, W, T), BF16),
+            pltpu.VMEM((2, 2, 2, W, T), F32),
             pltpu.SemaphoreType.DMA((24,)),
             pltpu.SemaphoreType.DMA((2, 2, 10)),
             pltpu.SemaphoreType.DMA((2, 2, 10)),

time: 46.9 us -> 45.1 us (0.962); the launches traced: 46.8 us -> 44.3 us
  Pallas kernels: 46.2 us -> 43.7 us
    pallas_call x1, Pallas kernels: 45.3 us -> 42.8 us  [body(): pl.pallas_call(kernel, out_shape=tuple((pltpu.VMEM(o.shape, o.dtype) for...]
where the time goes in v5:
time: 45.1 us; the launch traced here: 44.3 us
  Pallas kernels  43.7 us (97%)
  between operations  0.64 us (1%)
    pallas_call x1, Pallas kernels, body(): pl.pallas_call(kernel, out_shape=tuple((pltpu.VMEM(o.shape, o.dtype) for...  42.8 us

profile of v5, /device:TPU:0, one launch (start us, length us, event | category | flops | bytes accessed | tf_op | source)
XLA Modules:
  0.0 44.3 jit_solution(13715265121896690383)
XLA Ops:
  0.6 42.8 %shard_map.120 = (bf16[512,128]{1,0:T(8,128)(2,1)S(1)}, bf16[512,128]{1,0:T(8,128)(2,1)S(1)}, bf16[512,128]{1,0:T(8,128)(2,1)S(1)}, f32[256,256]{1,0:T(8,128)S(1)}) custom-call(bf16[512,128]{1,0:T(8,128)(2,1)} %bitcast.11, bf16[512,128]{1,0:T(8,128)(2,1)} %bitcast.12, bf16[512,128]{1,0:T(8,128)(2,1)} %bitcast.13, bf16[1024,128]{1,0:T(8,128)(2,1)} %bitcast.10, ...), custom_call_target="tpu_custom_call" | custom-call | tf_op jit(solution)/shard_map/pallas_call | solution.py:519
  43.4 0.9 %shard_map.121 = (bf16[512,128]{1,0:T(8,128)(2,1)}, bf16[512,128]{1,0:T(8,128)(2,1)}, bf16[512,128]{1,0:T(8,128)(2,1)}, f32[256,256]{1,0:T(8,128)}) custom-call(bf16[512,128]{1,0:T(8,128)(2,1)S(1)} %get-tuple-element.12.refs_0_, bf16[512,128]{1,0:T(8,128)(2,1)S(1)} %get-tuple-element.13.refs_1_, bf16[512,128]{1,0:T(8,128)(2,1)S(1)} %get-tuple-element.14.refs_2_, ...), custom_call_target="tpu_custom_call" | custom-call | tf_op jit(solution)/shard_map/pallas_call | solution.py:582

commit v6 on v5

--- a/solution.py
+++ b/solution.py
@@ -258,22 +258,10 @@
     pending = (jnp.int32(1), z, y)
 
     second = []
-    for some in (("q", "k"), ("v",), ("do", "st")):
-        for name in some:
-            for d in (0, 1):
-                first[d, name].wait_recv()
-                if d == (0 if name in ("q", "k") else 1):
-                    c = gather_copy(0, d, name, ring(0, -1 if d == 0 else 1), True)
-                    c.start()
-                    second.append(c)
-        z_arrived(some, False)
-        z_each(some, True, start)
-
-    for c in loads[8:]:
-        c.wait()
     rows = pl.ds(pl.multiple_of(core * 128, 128), 128)
     shares = []
-    for axis in (0, 1):
+
+    def share(axis):
         for role in (0, 1):
             step = role_step(axis, role)
             for w, owner in enumerate((ring(axis, step), ring(axis, 2))):
@@ -286,7 +274,39 @@
                 c.start()
                 shares.append(c)
 
-    pending = some_units(16, lambda n: (n // 8, (n % 8 + 1) // 3, (n % 8 + 1) % 3), pending, False)
+    def pass_on(some):
+        for name in some:
+            for d in (0, 1):
+                first[d, name].wait_recv()
+                if d == (0 if name in ("q", "k") else 1):
+                    c = gather_copy(0, d, name, ring(0, -1 if d == 0 else 1), True)
+                    c.start()
+                    second.append(c)
+
+    pass_on(("q", "k"))
+    for some in (("q", "k"), ("v",), ("do", "st")):
+        z_arrived(some, False)
+        z_each(some, True, start)
+    for c in loads[8:]:
+        c.wait()
+    share(1)
+    pending = some_units(
+        4, lambda n: (n // 2, jnp.where(n < 2, 0, n - 1), jnp.where(n < 2, n + 1, 0)), pending, False
+    )
+    pass_on(("v", "do", "st"))
+
+    share(0)
+
+    pending = some_units(
+        12,
+        lambda n: (
+            n // 6,
+            jnp.where(n < 6, n // 3 + 1, n % 3),
+            jnp.where(n < 6, n % 3, (n - 6) // 3 + 1),
+        ),
+        pending,
+        False,
+    )
     z_arrived(names, True)
     pending = some_units(
         6, lambda n: (n // 3, jnp.where(n < 3, n, 3), jnp.where(n < 3, 3, n - 3)), pending, False
@@ -396,29 +416,11 @@
     for h in both:
         dq[h].far()
     dq[0].direct()
-    for h in both:
-        dk[h].direct()
     pending = some_units(3, lambda n: (jnp.int32(1), n, jnp.int32(3)), pending, True)
     products(*pending)
     dq[1].direct()
     for h in both:
-        dk[h].far()
-    def block(h, owner, o):
-        return lat[o, owner] if h == 0 else lat[owner, o]
-
-    def term(h, role, w, owner, o):
-        near = dot(dqf[h], block(h, owner, 2 * role + o))
-        return near + dot(dqg[h, role], lx[h, role, w, o])
-
-    hands = {}
-    for h in both:
-        dqf[h] = dq[h].end().astype(BF16)
-        for role in both:
-            c = remote(
-                dqf.at[h], dqg.at[h, role], hs.at[h, role], hr.at[h, role], peer(h, role_step(h, role))
-            )
-            c.start()
-            hands[h, role] = c
+        dk[h].direct()
     swaps = []
     for c in shares:
         c.wait_recv()
@@ -428,16 +430,32 @@
             c = remote(ref, ref, ds.at[axis, role], dr.at[axis, role], sibling)
             c.start()
             swaps.append(c)
-    for h in both:
-        dk[h].summed()
-    for c in swaps:
-        c.wait_recv()
+    def block(h, owner, o):
+        return lat[o, owner] if h == 0 else lat[owner, o]
+
+    def term(h, role, w, owner, o):
+        near = dot(dqf[h], block(h, owner, 2 * role + o))
+        return near + dot(dqg[h, role], lx[h, role, w, o])
+
+    hands = {}
+    for h in both:
+        dqf[h] = dq[h].end().astype(BF16)
+        for role in both:
+            c = remote(
+                dqf.at[h], dqg.at[h, role], hs.at[h, role], hr.at[h, role], peer(h, role_step(h, role))
+            )
+            c.start()
+            hands[h, role] = c
+    for h in both:
+        dk[h].far()
     odd = [pos[1 - h] % 2 for h in both]
     trades = {}
     for h in both:
         for role in both:
             for n, o in enumerate((odd[h], 1 - odd[h])):
                 pre[h, role, n] = dot(dqf[h], block(h, ring(h, role_step(h, 1 - role)), 2 * role + o))
+    for c in swaps:
+        c.wait_recv()
     for n in both:
         for h in both:
             o = odd[h] if n == 0 else 1 - odd[h]
@@ -452,6 +470,9 @@
                 c.start()
                 trades[h, role, n] = c
 
+    for h in both:
+        dk[h].summed()
+
     def place(h, slot):
         return pl.ds(pl.multiple_of(slot * 128, 128), 128)
 
@@ -464,11 +485,6 @@
     for h in both:
         wide2[pl.ds(h, T, stride=2), :] = jnp.transpose(dqf[h].astype(F32))
     qg_ref[...] = wide2[0 : 2 * T, :].astype(BF16)
-    ends = [dk[h].end() for h in both]
-    for p, ref in ((0, kg_ref), (1, vg_ref)):
-        for h in both:
-            wide2[pl.ds(2 * T * p + h, T, stride=2), :] = ends[h][p]
-        ref[...] = wide2[2 * T * p : 2 * T * p + 2 * T, :].astype(BF16)
     for n in both:
         for h in both:
             o = odd[h] if n == 0 else 1 - odd[h]
@@ -481,6 +497,11 @@
                 wb[h].far()
             else:
                 wb[h].direct()
+    ends = [dk[h].end() for h in both]
+    for p, ref in ((0, kg_ref), (1, vg_ref)):
+        for h in both:
+            wide2[pl.ds(2 * T * p + h, T, stride=2), :] = ends[h][p]
+        ref[...] = wide2[2 * T * p : 2 * T * p + 2 * T, :].astype(BF16)
     for h in both:
         wg_ref[:, h * W : h * W + W] = jnp.transpose(wb[h].end())
 

time: 45.1 us -> 44.1 us (0.978); the launches traced: 44.3 us -> 44 us
  no operation moved by 1% of the time
where the time goes in v6:
time: 44.1 us; the launch traced here: 44 us
  Pallas kernels  43.3 us (98%)
  between operations  0.64 us (1%)
    pallas_call x1, Pallas kernels, body(): pl.pallas_call(kernel, out_shape=tuple((pltpu.VMEM(o.shape, o.dtype) for...  42.4 us

profile of v6, /device:TPU:0, one launch (start us, length us, event | category | flops | bytes accessed | tf_op | source)
XLA Modules:
  0.0 44.0 jit_solution(13501557700990027758)
XLA Ops:
  0.6 42.4 %shard_map.120 = (bf16[512,128]{1,0:T(8,128)(2,1)S(1)}, bf16[512,128]{1,0:T(8,128)(2,1)S(1)}, bf16[512,128]{1,0:T(8,128)(2,1)S(1)}, f32[256,256]{1,0:T(8,128)S(1)}) custom-call(bf16[512,128]{1,0:T(8,128)(2,1)} %bitcast.11, bf16[512,128]{1,0:T(8,128)(2,1)} %bitcast.12, bf16[512,128]{1,0:T(8,128)(2,1)} %bitcast.13, bf16[1024,128]{1,0:T(8,128)(2,1)} %bitcast.10, ...), custom_call_target="tpu_custom_call" | custom-call | tf_op jit(solution)/shard_map/pallas_call | solution.py:540
  43.1 0.9 %shard_map.121 = (bf16[512,128]{1,0:T(8,128)(2,1)}, bf16[512,128]{1,0:T(8,128)(2,1)}, bf16[512,128]{1,0:T(8,128)(2,1)}, f32[256,256]{1,0:T(8,128)}) custom-call(bf16[512,128]{1,0:T(8,128)(2,1)S(1)} %get-tuple-element.12.refs_0_, bf16[512,128]{1,0:T(8,128)(2,1)S(1)} %get-tuple-element.13.refs_1_, bf16[512,128]{1,0:T(8,128)(2,1)S(1)} %get-tuple-element.14.refs_2_, ...), custom_call_target="tpu_custom_call" | custom-call | tf_op jit(solution)/shard_map/pallas_call | solution.py:603

commit v7 on v6

--- a/solution.py
+++ b/solution.py
@@ -410,17 +410,22 @@
     wb = [Direct(btx, brx, 1 - h, 12, get_last(h)) for h in both]
 
     pending = some_units(
-        5, lambda n: (jnp.where(n == 0, 1, 0), jnp.int32(3), jnp.where(n == 0, 3, n - 1)), pending, False
+        8,
+        lambda n: (
+            jnp.where((n == 0) | (n > 4), 1, 0),
+            jnp.where(n > 4, n - 5, 3),
+            jnp.where((n == 0) | (n > 4), 3, n - 1),
+        ),
+        pending,
+        False,
     )
     products(*pending)
     for h in both:
         dq[h].far()
     dq[0].direct()
-    pending = some_units(3, lambda n: (jnp.int32(1), n, jnp.int32(3)), pending, True)
-    products(*pending)
     dq[1].direct()
     for h in both:
-        dk[h].direct()
+        dk[h].far()
     swaps = []
     for c in shares:
         c.wait_recv()
@@ -447,13 +452,15 @@
             c.start()
             hands[h, role] = c
     for h in both:
-        dk[h].far()
+        dk[h].direct()
     odd = [pos[1 - h] % 2 for h in both]
     trades = {}
     for h in both:
         for role in both:
             for n, o in enumerate((odd[h], 1 - odd[h])):
                 pre[h, role, n] = dot(dqf[h], block(h, ring(h, role_step(h, 1 - role)), 2 * role + o))
+    for h in both:
+        dk[h].summed()
     for c in swaps:
         c.wait_recv()
     for n in both:
@@ -469,9 +476,6 @@
                 )
                 c.start()
                 trades[h, role, n] = c
-
-    for h in both:
-        dk[h].summed()
 
     def place(h, slot):
         return pl.ds(pl.multiple_of(slot * 128, 128), 128)

time: 44.1 us -> 43.6 us (0.989)
    pallas_call x1, Pallas kernels: 42.4 us -> 42 us  [body(): pl.pallas_call(kernel, out_shape=tuple((pltpu.VMEM(o.shape, o.dtype) for...]
where the time goes in v7:
time: 43.6 us; the launch traced here: 43.5 us
  Pallas kernels  42.9 us (98%)
  between operations  0.64 us (1%)
    pallas_call x1, Pallas kernels, body(): pl.pallas_call(kernel, out_shape=tuple((pltpu.VMEM(o.shape, o.dtype) for...  42 us

profile of v7, /device:TPU:0, one launch (start us, length us, event | category | flops | bytes accessed | tf_op | source)
XLA Modules:
  0.0 43.5 jit_solution(17337783362733107237)
XLA Ops:
  0.6 42.0 %shard_map.120 = (bf16[512,128]{1,0:T(8,128)(2,1)S(1)}, bf16[512,128]{1,0:T(8,128)(2,1)S(1)}, bf16[512,128]{1,0:T(8,128)(2,1)S(1)}, f32[256,256]{1,0:T(8,128)S(1)}) custom-call(bf16[512,128]{1,0:T(8,128)(2,1)} %bitcast.11, bf16[512,128]{1,0:T(8,128)(2,1)} %bitcast.12, bf16[512,128]{1,0:T(8,128)(2,1)} %bitcast.13, bf16[1024,128]{1,0:T(8,128)(2,1)} %bitcast.10, ...), custom_call_target="tpu_custom_call" | custom-call | tf_op jit(solution)/shard_map/pallas_call | solution.py:544
  42.6 0.9 %shard_map.121 = (bf16[512,128]{1,0:T(8,128)(2,1)}, bf16[512,128]{1,0:T(8,128)(2,1)}, bf16[512,128]{1,0:T(8,128)(2,1)}, f32[256,256]{1,0:T(8,128)}) custom-call(bf16[512,128]{1,0:T(8,128)(2,1)S(1)} %get-tuple-element.12.refs_0_, bf16[512,128]{1,0:T(8,128)(2,1)S(1)} %get-tuple-element.13.refs_1_, bf16[512,128]{1,0:T(8,128)(2,1)S(1)} %get-tuple-element.14.refs_2_, ...), custom_call_target="tpu_custom_call" | custom-call | tf_op jit(solution)/shard_map/pallas_call | solution.py:607

commit v8 on v7

--- a/solution.py
+++ b/solution.py
@@ -137,13 +137,11 @@
     def wait_send(c):
         c.wait_send()
 
-    def send_own(some):
-        for name in some:
-            for d in (0, 1):
-                c = gather_copy(0, d, name, y, False)
-                c.start()
-                first[d, name] = c
-            z_each((name,), False, start)
+    def send_y(*some):
+        for d, name in some:
+            c = gather_copy(0, d, name, y, False)
+            c.start()
+            first[d, name] = c
 
     for n, (name, ref) in enumerate((("q", q_in), ("k", k_in), ("v", v_in))):
         loads[n].wait()
@@ -156,7 +154,8 @@
                 kv[h, kpos[h], n - 1] = part
         if n == 0:
             pl.semaphore_wait(barrier, 7)
-        send_own((name,))
+        send_y(*(((1, "v"), (0, "v")) if name == "v" else ((0, name),)))
+        z_each((name,), False, start)
 
     for c in loads[3:8]:
         c.wait()
@@ -182,7 +181,10 @@
         st[h, qpos[h], 2:3] = r1
         st[h, qpos[h], 3:4] = r2
         st[h, qpos[h], 4:8] = jnp.zeros((4, T), F32)
-    send_own(("do", "st"))
+    send_y((1, "do"), (1, "st"))
+    z_each(("do",), False, start)
+    z_each(("st",), False, start)
+    send_y((1, "q"), (1, "k"), (0, "do"), (0, "st"))
 
     dqt[...] = jnp.zeros_like(dqt)
     dkv[...] = jnp.zeros_like(dkv)
@@ -274,16 +276,11 @@
                 c.start()
                 shares.append(c)
 
-    def pass_on(some):
-        for name in some:
-            for d in (0, 1):
-                first[d, name].wait_recv()
-                if d == (0 if name in ("q", "k") else 1):
-                    c = gather_copy(0, d, name, ring(0, -1 if d == 0 else 1), True)
-                    c.start()
-                    second.append(c)
-
-    pass_on(("q", "k"))
+    for d, name in ((0, "q"), (1, "v"), (0, "k"), (1, "do"), (1, "st")):
+        first[d, name].wait_recv()
+        c = gather_copy(0, d, name, ring(0, -1 if d == 0 else 1), True)
+        c.start()
+        second.append(c)
     for some in (("q", "k"), ("v",), ("do", "st")):
         z_arrived(some, False)
         z_each(some, True, start)
@@ -293,7 +290,8 @@
     pending = some_units(
         4, lambda n: (n // 2, jnp.where(n < 2, 0, n - 1), jnp.where(n < 2, n + 1, 0)), pending, False
     )
-    pass_on(("v", "do", "st"))
+    for d, name in ((1, "q"), (1, "k"), (0, "v"), (0, "do"), (0, "st")):
+        first[d, name].wait_recv()
 
     share(0)
 
@@ -451,8 +449,6 @@
             )
             c.start()
             hands[h, role] = c
-    for h in both:
-        dk[h].direct()
     odd = [pos[1 - h] % 2 for h in both]
     trades = {}
     for h in both:
@@ -476,6 +472,9 @@
                 )
                 c.start()
                 trades[h, role, n] = c
+
+    for h in both:
+        dk[h].direct()
 
     def place(h, slot):
         return pl.ds(pl.multiple_of(slot * 128, 128), 128)

time: 43.6 us -> 43.7 us (level)
  no operation moved by 1% of the time
where the time goes in v8:
time: 43.7 us; the launch traced here: 43.6 us
  Pallas kernels  43 us (98%)
  between operations  0.64 us (1%)
    pallas_call x1, Pallas kernels, body(): pl.pallas_call(kernel, out_shape=tuple((pltpu.VMEM(o.shape, o.dtype) for...  42.1 us

profile of v8, /device:TPU:0, one launch (start us, length us, event | category | flops | bytes accessed | tf_op | source)
XLA Modules:
  0.0 43.6 jit_solution(6007722639524749451)
XLA Ops:
  0.6 42.1 %shard_map.120 = (bf16[512,128]{1,0:T(8,128)(2,1)S(1)}, bf16[512,128]{1,0:T(8,128)(2,1)S(1)}, bf16[512,128]{1,0:T(8,128)(2,1)S(1)}, f32[256,256]{1,0:T(8,128)S(1)}) custom-call(bf16[512,128]{1,0:T(8,128)(2,1)} %bitcast.11, bf16[512,128]{1,0:T(8,128)(2,1)} %bitcast.12, bf16[512,128]{1,0:T(8,128)(2,1)} %bitcast.13, bf16[1024,128]{1,0:T(8,128)(2,1)} %bitcast.10, ...), custom_call_target="tpu_custom_call" | custom-call | tf_op jit(solution)/shard_map/pallas_call | solution.py:543
  42.7 0.9 %shard_map.121 = (bf16[512,128]{1,0:T(8,128)(2,1)}, bf16[512,128]{1,0:T(8,128)(2,1)}, bf16[512,128]{1,0:T(8,128)(2,1)}, f32[256,256]{1,0:T(8,128)}) custom-call(bf16[512,128]{1,0:T(8,128)(2,1)S(1)} %get-tuple-element.12.refs_0_, bf16[512,128]{1,0:T(8,128)(2,1)S(1)} %get-tuple-element.13.refs_1_, bf16[512,128]{1,0:T(8,128)(2,1)S(1)} %get-tuple-element.14.refs_2_, ...), custom_call_target="tpu_custom_call" | custom-call | tf_op jit(solution)/shard_map/pallas_call | solution.py:606
